TPU v7x, 256 devices: a whole 4x4x8 slice. The times are simulated.
256 devices in a mesh: ep: 64 (over z, x, core), tp: 4 (over y).
Axes of the slice: x: 4, y: 4, z: 8, core: 2. Of those that a mesh axis runs over, the one named last changes fastest.
Arguments:
- residual_in: bfloat16 [1024, 2048], P('ep'), may hold values from -6 to 6
- lengths: int32 [1024], P('ep'), may hold values from 1 to 511, as said below
- kv_cache: bfloat16 [1024, 4, 512, 256], P('ep', 'tp'), may hold values from -640 to 640
- norm_gain_attn: float32 [2048], replicated, may hold values from 0.1 to 1.9
- query_weight: bfloat16 [2048, 2048], P(None, 'tp'), may hold values from -0.125 to 0.125
- key_weight: bfloat16 [2048, 512], P(None, 'tp'), may hold values from -0.125 to 0.125
- value_weight: bfloat16 [2048, 512], P(None, 'tp'), may hold values from -0.125 to 0.125
- diff_lambda: float32 [16], P('tp'), may hold values from 0.3 to 0.8
- head_gain: float32 [128], replicated, may hold values from 0.1 to 1.9
- out_weight: bfloat16 [2048, 2048], P(None, 'tp'), may hold values from -0.125 to 0.125
- norm_gain_ffn: float32 [2048], replicated, may hold values from 0.1 to 1.9
- route_ids: int32 [1024, 2], P('ep'), may hold values from 0 to 63, as said below
- route_weights: float32 [1024, 2], P('ep'), may hold values from 0.1 to 1
- expert_gate: bfloat16 [64, 2048, 512], P('ep', None, 'tp'), may hold values from -0.125 to 0.125
- expert_up: bfloat16 [64, 2048, 512], P('ep', None, 'tp'), may hold values from -0.125 to 0.125
- expert_down: bfloat16 [64, 512, 2048], P('ep', 'tp'), may hold values from -0.25 to 0.25
- dense_gate: bfloat16 [2048, 8192], P(None, 'ep'), may hold values from -0.125 to 0.125
- dense_up: bfloat16 [2048, 8192], P(None, 'ep'), may hold values from -0.125 to 0.125
- dense_down: bfloat16 [8192, 2048], P('ep'), may hold values from -0.0625 to 0.0625
- dense_mix: float32 [2048], replicated, may hold values from -0.125 to 0.125
Outputs:
- layer_out: bfloat16 [1024, 2048], P('ep', 'tp')
- new_rows: bfloat16 [1024, 4, 256], P('ep', 'tp')
Inputs may be any that keep to these rules, and one draw needn't show every extreme that they name: The new token stands at position lengths[b]; some sequence holds 511 positions in every draw. `route_ids`: each row names 2 different experts from one group; the groups are the 4 runs of consecutive expert numbers of equal size. Among the rows of one index of ep no expert is named more than 2 times, and some expert exactly 2 times.
All inputs are finite; a program needn't handle non-finite values.
Results may differ from a plain program's by a relative error of at most 0.008.
The roundings to bfloat16 on the way count: a program that leaves them out, or rounds other values in their place, can miss the bound.
Values may be sent and summed in bfloat16 or wider, within the bound.
A program may use at most 64 MiB of HBM per device.

v0:
```python
import jax
import jax.numpy as jnp
from jax import lax
from jax.sharding import PartitionSpec as P

QK_DIM = 64
HEAD_DIM = 128
TOPK = 2


EPS = 1e-06


def from_everyone(array, axis):
    copies = jnp.broadcast_to(array, (lax.axis_size(axis), *array.shape))
    return lax.all_to_all(copies, axis, split_axis=0, concat_axis=0, tiled=True)


def in_order(pieces, dim):
    pieces = jnp.moveaxis(pieces, 0, dim)
    lengths = pieces.shape
    return pieces.reshape(*lengths[:dim], lengths[dim] * lengths[dim + 1], *lengths[dim + 2 :])


def gather_directly(array, axis, dim):
    pieces = from_everyone(array, axis)
    return in_order(pieces, dim)


def split_up(array, dim, peers):
    lengths = array.shape
    pieces = array.reshape(*lengths[:dim], peers, lengths[dim] // peers, *lengths[dim + 1 :])
    return jnp.moveaxis(pieces, dim, 0)


def summed_on_arrival(array, axis, dim):
    pieces = split_up(array, dim, lax.axis_size(axis))
    arrived = lax.all_to_all(pieces, axis, split_axis=0, concat_axis=0, tiled=True)
    return arrived.astype(jnp.float32).sum(axis=0)


def rms_rows(values, gain):
    mean_sq = jnp.mean(values * values, axis=-1, keepdims=True)
    return values * lax.rsqrt(mean_sq + EPS) * gain


def rotate(vectors, positions):
    half = vectors.shape[-1] // 2
    inverse = 10000.0 ** (-jnp.arange(half, dtype=jnp.float32) / half)
    angle = positions[:, None, None, None] * inverse
    cosine = jnp.cos(angle)
    sine = jnp.sin(angle)
    first = vectors[..., :half]
    second = vectors[..., half:]
    return jnp.concatenate(
        [first * cosine - second * sine, first * sine + second * cosine], axis=-1
    )


def normalize(scores, latest, valid):
    masked = jnp.where(valid, scores, -jnp.inf)
    top = jnp.maximum(jnp.max(masked, axis=-1), latest)
    raised = jnp.where(valid, jnp.exp(jnp.where(valid, scores, 0.0) - top[..., None]), 0.0)
    raised_new = jnp.exp(latest - top)
    total = jnp.sum(raised, axis=-1) + raised_new
    return (raised / total[..., None], raised_new / total)


def attend(query, fresh, cache, lengths, lam):
    count = fresh.shape[0]
    groups = fresh.shape[1]
    share = query.shape[1] // groups
    scale = QK_DIM ** (-0.5)
    grouped = query.reshape(count, groups, share, 2, QK_DIM)
    first = (
        jnp.einsum(
            "bgjd,bgkd->bgjk",
            grouped[:, :, :, 0],
            cache[..., :QK_DIM],
            preferred_element_type=jnp.float32,
        )
        * scale
    )
    second = (
        jnp.einsum(
            "bgjd,bgkd->bgjk",
            grouped[:, :, :, 1],
            cache[..., QK_DIM : 2 * QK_DIM],
            preferred_element_type=jnp.float32,
        )
        * scale
    )
    first_new = (
        jnp.einsum(
            "bgjd,bgd->bgj",
            grouped[:, :, :, 0],
            fresh[..., :QK_DIM],
            preferred_element_type=jnp.float32,
        )
        * scale
    )
    second_new = (
        jnp.einsum(
            "bgjd,bgd->bgj",
            grouped[:, :, :, 1],
            fresh[..., QK_DIM : 2 * QK_DIM],
            preferred_element_type=jnp.float32,
        )
        * scale
    )
    valid = (
        jnp.arange(cache.shape[2], dtype=jnp.int32)[None, None, None, :]
        < lengths[:, None, None, None]
    )
    prob_one, prob_one_new = normalize(first, first_new, valid)
    prob_two, prob_two_new = normalize(second, second_new, valid)
    weight = lam.reshape(groups, share)[None, :, :, None]
    mapped = (prob_one - weight * prob_two).astype(jnp.bfloat16)
    mapped_new = (prob_one_new - weight[..., 0] * prob_two_new).astype(jnp.bfloat16)
    output = jnp.einsum(
        "bgjk,bgkd->bgjd", mapped, cache[..., 2 * QK_DIM :], preferred_element_type=jnp.float32
    )
    output = output + mapped_new.astype(jnp.float32)[..., None] * fresh[
        :, :, None, 2 * QK_DIM :
    ].astype(jnp.float32)
    return output.reshape(count, groups * share, HEAD_DIM)


def on_device(
    residual_in,
    lengths,
    kv_cache,
    norm_gain_attn,
    query_weight,
    key_weight,
    value_weight,
    diff_lambda,
    head_gain,
    out_weight,
    norm_gain_ffn,
    route_ids,
    route_weights,
    expert_gate,
    expert_up,
    expert_down,
    dense_gate,
    dense_up,
    dense_down,
    dense_mix,
):
    seq_count, width = residual_in.shape
    lanes = lax.axis_size("tp")
    column = lax.axis_index("tp")
    quarter = width // lanes
    groups = kv_cache.shape[1]
    local_heads = diff_lambda.shape[0]
    resid = residual_in.astype(jnp.float32)
    normed = rms_rows(resid, norm_gain_attn).astype(jnp.bfloat16)
    positions = lengths.astype(jnp.float32)
    query = jnp.dot(normed, query_weight, preferred_element_type=jnp.float32).reshape(
        seq_count, local_heads, 2, QK_DIM
    )
    query = rotate(query, positions).astype(jnp.bfloat16)
    keys = jnp.dot(normed, key_weight, preferred_element_type=jnp.float32).reshape(
        seq_count, groups, 2, QK_DIM
    )
    keys = rotate(keys, positions).astype(jnp.bfloat16).reshape(seq_count, groups, 2 * QK_DIM)
    values = (
        jnp.dot(normed, value_weight, preferred_element_type=jnp.float32)
        .reshape(seq_count, groups, HEAD_DIM)
        .astype(jnp.bfloat16)
    )
    fresh = jnp.concatenate([keys, values], axis=-1)
    mixed = attend(query, fresh, kv_cache, lengths, diff_lambda)
    heads_out = (
        rms_rows(mixed, head_gain).astype(jnp.bfloat16).reshape(seq_count, local_heads * HEAD_DIM)
    )
    all_heads = gather_directly(heads_out, "tp", 1)
    attn_cols = jnp.dot(all_heads, out_weight, preferred_element_type=jnp.float32)
    own_cols = lax.dynamic_slice_in_dim(resid, column * quarter, quarter, 1)
    stream_cols = (own_cols + attn_cols).astype(jnp.bfloat16)
    stream = gather_directly(stream_cols, "tp", 1)
    ffn_in = rms_rows(stream.astype(jnp.float32), norm_gain_ffn).astype(jnp.bfloat16)
    held = expert_gate.shape[0]
    expert_total = lax.axis_size("ep") * held
    capacity = max(2, 2 * TOPK * seq_count // expert_total)
    flat_ids = route_ids.reshape(-1)
    member = (flat_ids[:, None] == jnp.arange(expert_total, dtype=jnp.int32)[None, :]).astype(
        jnp.int32
    )
    slot = jnp.sum((jnp.cumsum(member, axis=0) - member) * member, axis=1)
    target = (flat_ids * capacity + slot).reshape(seq_count, TOPK)
    picker = (
        target[None, :, :] == jnp.arange(expert_total * capacity, dtype=jnp.int32)[:, None, None]
    )
    picker = jnp.any(picker, axis=2).astype(jnp.bfloat16)
    outgoing = jnp.dot(picker, ffn_in, preferred_element_type=jnp.float32).astype(jnp.bfloat16)
    outgoing = outgoing.reshape(expert_total, capacity, ffn_in.shape[1])
    arrived = lax.all_to_all(outgoing, "ep", split_axis=0, concat_axis=0, tiled=True)
    senders = arrived.shape[0] // held
    blocked = arrived.reshape(senders, held, arrived.shape[1], width)
    gate = jnp.einsum("sjcd,jdf->sjcf", blocked, expert_gate, preferred_element_type=jnp.float32)
    upward = jnp.einsum("sjcd,jdf->sjcf", blocked, expert_up, preferred_element_type=jnp.float32)
    hidden = (jax.nn.silu(gate) * upward).astype(jnp.bfloat16)
    partial_out = jnp.einsum(
        "sjcf,jfd->sjcd", hidden, expert_down, preferred_element_type=jnp.float32
    )
    partial_out = partial_out.reshape(arrived.shape[0], arrived.shape[1], width)
    summed = summed_on_arrival(partial_out.astype(jnp.bfloat16), "tp", 2)
    returned = lax.all_to_all(
        summed.astype(jnp.bfloat16), "ep", split_axis=0, concat_axis=0, tiled=True
    )
    flat_back = returned.reshape(expert_total * capacity, quarter)
    picked = flat_back[target]
    expert_cols = jnp.sum(route_weights[..., None] * picked.astype(jnp.float32), axis=1)
    gate_mix = jax.nn.sigmoid(jnp.sum(ffn_in.astype(jnp.float32) * dense_mix, axis=-1))
    piece = lax.all_gather(ffn_in, "ep", axis=0, tiled=True)
    gate = jnp.dot(piece, dense_gate, preferred_element_type=jnp.float32)
    upward = jnp.dot(piece, dense_up, preferred_element_type=jnp.float32)
    dense_hidden = (jax.nn.silu(gate) * upward).astype(jnp.bfloat16)
    down_part = lax.dynamic_slice_in_dim(dense_down, column * quarter, quarter, 1)
    dense_cols = summed_on_arrival(
        jnp.dot(dense_hidden, down_part, preferred_element_type=jnp.float32).astype(jnp.bfloat16),
        "ep",
        0,
    )
    layer_out = (
        stream_cols.astype(jnp.float32) + expert_cols + gate_mix[:, None] * dense_cols
    ).astype(jnp.bfloat16)
    return (layer_out, fresh)


def solution(mesh):
    placed = (
        P("ep", None),
        P("ep"),
        P("ep", "tp", None, None),
        P(),
        P(None, "tp"),
        P(None, "tp"),
        P(None, "tp"),
        P("tp"),
        P(),
        P(None, "tp"),
        P(),
        P("ep", None),
        P("ep", None),
        P("ep", None, "tp"),
        P("ep", None, "tp"),
        P("ep", "tp", None),
        P(None, "ep"),
        P(None, "ep"),
        P("ep", None),
        P(),
    )
    return jax.shard_map(
        on_device,
        mesh=mesh,
        in_specs=placed,
        out_specs=(P("ep", "tp"), P("ep", "tp", None)),
        check_vma=False,
    )
```

profile of v0, /device:TPU:1, one launch (start us, length us, event | category | flops | bytes accessed | tf_op | source)
XLA Modules:
  0.0 177.4 jit_solution(7542298937267518820)
XLA Ops:
  7.2 0.8 convert_element_type.131
  8.0 0.7 iota_compare_fusion
  8.7 1.0 multiply_reduce_fusion.1
  9.7 0.7 broadcast_bitcast_fusion
  10.4 1.3 fusion.73
  11.8 1.3 fusion.76
  13.6 1.3 fusion.74
  15.4 2.5 %fusion.12 = f32[16,4,512]{2,1,0:T(4,128)S(1)} fusion(bf16[16,4,64]{2,1,0:T(4,128)(2,1)S(1)} %get-tuple-element.10, bf16[16,1,512,256]{3,2,1,0:T(8,128)(2,1)} %param.22), kind=kOutput, calls=%fused_computation.17 | convolution fusion | flops 4227072 | bytes 2236416 | tf_op jit(solution)/shard_map/bgjd,bgkd->bgjk/dot_general | solution.py:85
  18.1 2.3 %select_reduce_fusion.1 = (f32[16,4]{1,0:T(8,128)S(1)}, f32[16,4]{1,0:T(8,128)S(1)}, f32[16,4,512]{2,1,0:T(4,128)S(1)}) fusion(pred[16,512]{1,0:T(8,128)(4,1)S(1)} %iota_compare_fusion, f32[16,4,512]{2,1,0:T(4,128)S(1)} %fusion.12, bf16[16,4,64]{2,1,0:T(4,128)(2,1)S(1)} %get-tuple-element.11, bf16[16,1,512,256]{3,2,1,0:T(8,128)(2,1)} %param.22), kind=kOutput, calls=%fused_computation.52 | convolution fusion | flops 4358016 | bytes 2376192 | tf_op jit(solution)/shard_map/bgjd,bgkd->bgjk/dot_general | solution.py:76
  20.8 0.6 multiply_reduce_fusion.3
  21.5 0.6 broadcast_in_dim.69
  22.1 5.0 %all-to-all-start = ((bf16[4,16,512]{2,1,0:T(8,128)(2,1)}), bf16[4,16,512]{2,1,0:T(8,128)(2,1)S(1)}, u32[]{:S(2)}, u32[]{:S(2)}) async-start(bf16[4,16,512]{2,1,0:T(8,128)(2,1)} %broadcast_in_dim.69), calls=%async_computation | async-start | bytes 131072 | tf_op jit(solution)/shard_map/all_to_all | solution.py:16
  27.1 4.5 %all-to-all-done = bf16[4,16,512]{2,1,0:T(8,128)(2,1)S(1)} async-done(((bf16[4,16,512]{2,1,0:T(8,128)(2,1)}), bf16[4,16,512]{2,1,0:T(8,128)(2,1)S(1)}, u32[]{:S(2)}, u32[]{:S(2)}) %all-to-all-start) | async-done | bytes 65568 | tf_op jit(solution)/shard_map/all_to_all | solution.py:16
  31.6 2.0 %fusion.19 = bf16[16,512]{1,0:T(8,128)(2,1)S(1)} fusion(bf16[16,2048]{1,0:T(8,128)(2,1)S(1)} %bitcast.127, bf16[2048,512]{1,0:T(8,128)(2,1)} %param.29, f32[16,2048]{1,0:T(8,128)S(1)} %convert_element_type.129, s32[]{:T(128)S(6)} %select_n.32), kind=kOutput, calls=%fused_computation.25 | convolution fusion | flops 33570816 | bytes 2211844 | tf_op jit(solution)/shard_map/dot_general | solution.py:179
  33.6 6.8 %all_to_all.30 = bf16[4,16,512]{2,1,0:T(8,128)(2,1)S(1)} all-to-all(bf16[4,16,512]{2,1,0:T(8,128)(2,1)S(1)} %broadcast_in_dim.70), channel_id=1, replica_groups=mesh['ep'=64,'tp'=4] {'tp'}, dimensions={0} | all-to-all | bytes 131072 | tf_op jit(solution)/shard_map/all_to_all | solution.py:16
  40.6 0.7 multiply_convert_fusion
  42.1 1.2 convolution_convert_fusion.1
  43.7 33.7 %all_to_all.31 = bf16[64,2,2048]{2,1,0:T(2,128)(2,1)S(1)} all-to-all(bf16[64,2,2048]{2,1,0:T(2,128)(2,1)S(1)} %reshape.369), channel_id=1, replica_groups=mesh['ep'=64,'tp'=4] {'ep'}, dimensions={0} | all-to-all | bytes 1048576 | tf_op jit(solution)/shard_map/all_to_all | solution.py:199
  77.3 1.4 convolution_bitcast_fusion.1
  78.7 1.8 %fusion = bf16[64,1,2,2048]{3,0,2,1:T(8,128)(2,1)S(1)} fusion(bf16[1,128,2048]{2,1,0:T(8,128)(2,1)} %param.35, bf16[1,2048,128]{2,1,0:T(8,128)(2,1)} %param.34, bf16[64,2,2048]{2,1,0:T(2,128)(2,1)S(1)} %all_to_all.31, f32[64,1,2,128]{3,0,2,1:T(8,128)S(1)} %convolution_bitcast_fusion.1), kind=kOutput, calls=%fused_computation.3 | convolution fusion | flops 134578176 | bytes 2162688 | tf_op jit(solution)/shard_map/sjcf,jfd->sjcd/dot_general | solution.py:205
  80.5 0.4 convert_element_type.153
  81.0 11.8 %all_to_all.32 = bf16[4,64,2,512]{3,1,2,0:T(8,128)(2,1)S(1)} all-to-all(bf16[4,64,2,512]{3,1,2,0:T(8,128)(2,1)S(1)} %bitcast.123), channel_id=1, replica_groups=mesh['ep'=64,'tp'=4] {'tp'}, dimensions={0} | all-to-all | bytes 1048576 | tf_op jit(solution)/shard_map/all_to_all | solution.py:38
  92.9 0.8 copy.105
  93.6 6.3 %all-to-all-start.4 = ((bf16[64,2,512]{2,1,0:T(2,128)(2,1)}), bf16[64,2,512]{2,1,0:T(2,128)(2,1)S(1)}, u32[]{:S(2)}, u32[]{:S(2)}) async-start(bf16[64,2,512]{2,1,0:T(2,128)(2,1)} %copy.105), calls=%async_computation.4 | async-start | bytes 262144 | tf_op jit(solution)/shard_map/all_to_all | solution.py:210
  99.9 26.2 %all-gather.2.cloned.1.call-done = bf16[1024,2048]{1,0:T(8,128)(2,1)} async-done(((bf16[16,2048]{1,0:T(8,128)(2,1)}), bf16[1024,2048]{1,0:T(8,128)(2,1)}) %all-gather.2.cloned.1.call-update) | async-done | bytes 4194320 | tf_op jit(solution)/shard_map/all_gather | solution.py:217
  126.1 3.4 %fusion.77 = f32[1024,128]{1,0:T(8,128)S(1)} fusion(bf16[1024,2048]{1,0:T(8,128)(2,1)} %all-gather.2.cloned.1.call-done, bf16[2048,128]{1,0:T(8,128)(2,1)S(1)} %copy-done.3), kind=kOutput, calls=%fused_computation.130 | convolution fusion | flops 536870912 | bytes 5242880 | tf_op jit(solution)/shard_map/dot_general | solution.py:218
  129.6 5.3 %convolution_convert_fusion.2 = bf16[1024,512]{1,0:T(8,128)(2,1)} fusion(bf16[1024,2048]{1,0:T(8,128)(2,1)} %all-gather.2.cloned.1.call-done, bf16[2048,128]{1,0:T(8,128)(2,1)} %param.37, f32[1024,128]{1,0:T(8,128)S(1)} %fusion.77, bf16[128,2048]{1,0:T(8,128)(2,1)} %param.38, s32[]{:T(128)S(6)} %select_n.32), kind=kOutput, calls=%fused_computation.13 | convolution fusion | flops 672399360 | bytes 6422532 | tf_op jit(solution)/shard_map/dot_general | solution.py:223
  134.8 6.7 %all-to-all-start.5 = ((bf16[64,16,512]{2,1,0:T(8,128)(2,1)}), bf16[64,16,512]{2,1,0:T(8,128)(2,1)S(1)}, u32[]{:S(2)}, u32[]{:S(2)}) async-start(bf16[64,16,512]{2,1,0:T(8,128)(2,1)} %bitcast.125), calls=%async_computation.5 | async-start | bytes 2097152 | tf_op jit(solution)/shard_map/all_to_all | solution.py:38
  141.8 0.6 pad_maximum_fusion.2
  142.7 0.6 gather_fusion
  143.6 26.1 %all-to-all-done.5 = bf16[64,16,512]{2,1,0:T(8,128)(2,1)S(1)} async-done(((bf16[64,16,512]{2,1,0:T(8,128)(2,1)}), bf16[64,16,512]{2,1,0:T(8,128)(2,1)S(1)}, u32[]{:S(2)}, u32[]{:S(2)}) %all-to-all-start.5) | async-done | bytes 1048608 | tf_op jit(solution)/shard_map/all_to_all | solution.py:38
  169.9 0.7 add_convert_fusion.1
  (72 shorter events, 4.1 us)
Async XLA Ops:
  7.2 6.4 %copy-start = (bf16[2048,512]{1,0:T(8,128)(2,1)S(1)}, bf16[2048,512]{1,0:T(8,128)(2,1)}, u32[]{:S(2)}) copy-start(bf16[2048,512]{1,0:T(8,128)(2,1)} %param.24) | copy-start | bytes 6291460
  15.4 5.3 %copy-start.8 = (f32[4]{0:T(128)S(1)}, f32[4]{0:T(128)}, u32[]{:S(2)}) copy-start(f32[4]{0:T(128)} %param.27) | copy-start | bytes 52
  15.4 5.3 %copy-start.2 = (bf16[16,1,512,256]{3,2,1,0:T(8,128)(2,1)S(1)}, bf16[16,1,512,256]{3,2,1,0:T(8,128)(2,1)}, u32[]{:S(2)}) copy-start(bf16[16,1,512,256]{3,2,1,0:T(8,128)(2,1)} %param.22) | copy-start | bytes 12582916
  20.8 6.4 %copy-start.1 = (bf16[16,2048]{1,0:T(8,128)(2,1)S(1)}, bf16[16,2048]{1,0:T(8,128)(2,1)}, u32[]{:S(2)}) copy-start(bf16[16,2048]{1,0:T(8,128)(2,1)} %param.20) | copy-start | bytes 196612
  21.4 19.2 %copy-start.4 = (f32[2048]{0:T(1024)S(1)}, f32[2048]{0:T(1024)}, u32[]{:S(2)}) copy-start(f32[2048]{0:T(1024)} %param.30) | copy-start | bytes 24580
  21.4 20.0 %copy-start.6 = (s32[16,2]{0,1:T(2,128)S(1)}, s32[16,2]{0,1:T(2,128)}, u32[]{:S(2)}) copy-start(s32[16,2]{0,1:T(2,128)} %param.31) | copy-start | bytes 388
  22.1 9.5 %all-to-all-start = ((bf16[4,16,512]{2,1,0:T(8,128)(2,1)}), bf16[4,16,512]{2,1,0:T(8,128)(2,1)S(1)}, u32[]{:S(2)}, u32[]{:S(2)}) async-start(bf16[4,16,512]{2,1,0:T(8,128)(2,1)} %broadcast_in_dim.69), calls=%async_computation | async-start | bytes 131072 | tf_op jit(solution)/shard_map/all_to_all | solution.py:16
  27.1 99.0 %all-gather.2.cloned.1.call-start = ((), (), s32[]{:S(2)}) async-start(), calls=%async_computation.6 | async-start | bytes 4259840 | tf_op jit(solution)/shard_map/all_gather | solution.py:217
  80.9 45.2 %copy-start.3 = (bf16[2048,128]{1,0:T(8,128)(2,1)S(1)}, bf16[2048,128]{1,0:T(8,128)(2,1)}, u32[]{:S(2)}) copy-start(bf16[2048,128]{1,0:T(8,128)(2,1)} %param.36) | copy-start | bytes 1572868
  93.6 41.2 %all-to-all-start.4 = ((bf16[64,2,512]{2,1,0:T(2,128)(2,1)}), bf16[64,2,512]{2,1,0:T(2,128)(2,1)S(1)}, u32[]{:S(2)}, u32[]{:S(2)}) async-start(bf16[64,2,512]{2,1,0:T(2,128)(2,1)} %copy.105), calls=%async_computation.4 | async-start | bytes 262144 | tf_op jit(solution)/shard_map/all_to_all | solution.py:210
  134.8 6.7 %copy-start.7 = (f32[16,2]{0,1:T(2,128)S(1)}, f32[16,2]{0,1:T(2,128)}, u32[]{:S(2)}) copy-start(f32[16,2]{0,1:T(2,128)} %param.32) | copy-start | bytes 388
  134.8 6.8 %copy-start.5 = (f32[2048]{0:T(1024)S(1)}, f32[2048]{0:T(1024)}, u32[]{:S(2)}) copy-start(f32[2048]{0:T(1024)} %param.39) | copy-start | bytes 24580
  134.8 34.9 %all-to-all-start.5 = ((bf16[64,16,512]{2,1,0:T(8,128)(2,1)}), bf16[64,16,512]{2,1,0:T(8,128)(2,1)S(1)}, u32[]{:S(2)}, u32[]{:S(2)}) async-start(bf16[64,16,512]{2,1,0:T(8,128)(2,1)} %bitcast.125), calls=%async_computation.5 | async-start | bytes 2097152 | tf_op jit(solution)/shard_map/all_to_all | solution.py:38
Sparse Core Ops, SparseCore 0:
  41.5 84.6 all-gather.1
where the time goes:
time: 178 us; the launch traced here: 177 us
  waiting for transfers between devices  56.8 us (32%)
  blocking collectives  52.3 us (29%)
  matrix products  24.6 us (14%)
  starting transfers between devices  18 us (10%)
  between operations  14.3 us (8%)
  other arithmetic  6.57 us (4%)
  local copies, waits for them, and re-layouts  4.77 us (3%)
    all_to_all x1, blocking collectives, on_device(): lax.all_to_all(outgoing, 'ep', split_axis=0, concat_axis=0, tiled=True)  33.7 us
    all_gather x1, waiting for transfers between devices, on_device(): piece = lax.all_gather(ffn_in, 'ep', axis=0, tiled=True)  26.2 us
    all_to_all x1, waiting for transfers between devices, summed_on_arrival(): lax.all_to_all(pieces, axis, split_axis=0, concat_axis=0, tiled=True)  26.1 us
    all_to_all x1, blocking collectives, summed_on_arrival(): lax.all_to_all(pieces, axis, split_axis=0, concat_axis=0, tiled=True)  11.8 us
    all_to_all x1, blocking collectives, from_everyone(): return lax.all_to_all(copies, axis, split_axis=0, concat_axis=0, tiled=True)  6.84 us
    all_to_all x1, starting transfers between devices, summed_on_arrival(): lax.all_to_all(pieces, axis, split_axis=0, concat_axis=0, tiled=True)  6.69 us
    all_to_all x1, starting transfers between devices, on_device(): lax.all_to_all(summed.astype(jnp.bfloat16), 'ep', split_axis=0, concat_ax...  6.29 us
    dot_general x1, matrix products, on_device(): jnp.dot(dense_hidden, down_part, preferred_element_type=jnp.float32)  5.25 us
  transfers between devices with their start and end apart: 4, of which 3 were waited for; matrix products, arithmetic and copies ran while one was open for 10% of the time, Pallas kernels for 0%

commit v1 on v0

v1 whole, which is shorter than its diff:
```python
import jax
import jax.numpy as jnp
from jax import lax
from jax.experimental import pallas as pl
from jax.experimental.pallas import tpu as pltpu
from jax.sharding import PartitionSpec as P

QK_DIM = 64
HEAD_DIM = 128
EPS = 1e-06
MESH = pl.DeviceIdType.MESH
F32 = jnp.float32
BF16 = jnp.bfloat16
NX, NZ, NY, NC = 4, 8, 4, 2
SEQ = 16
D = 2048
Q = 512
INFO = 128
WIDE = D + INFO
FF = 128
X_ORDER = (0, 1, 3, 2)
N_SENDS = 63


def rms_rows(values, gain):
    mean_sq = jnp.mean(values * values, axis=-1, keepdims=True)
    return values * lax.rsqrt(mean_sq + EPS) * gain


def rotate(vectors, positions):
    half = vectors.shape[-1] // 2
    inverse = 10000.0 ** (-jnp.arange(half, dtype=jnp.float32) / half)
    angle = positions[:, None, None, None] * inverse
    cosine = jnp.cos(angle)
    sine = jnp.sin(angle)
    first = vectors[..., :half]
    second = vectors[..., half:]
    return jnp.concatenate(
        [first * cosine - second * sine, first * sine + second * cosine], axis=-1
    )


def normalize(scores, latest, valid):
    masked = jnp.where(valid, scores, -jnp.inf)
    top = jnp.maximum(jnp.max(masked, axis=-1), latest)
    raised = jnp.where(valid, jnp.exp(jnp.where(valid, scores, 0.0) - top[..., None]), 0.0)
    raised_new = jnp.exp(latest - top)
    total = jnp.sum(raised, axis=-1) + raised_new
    return (raised / total[..., None], raised_new / total)


def attend(query, fresh, cache, lengths, lam):
    count = fresh.shape[0]
    groups = fresh.shape[1]
    share = query.shape[1] // groups
    scale = QK_DIM ** (-0.5)
    grouped = query.reshape(count, groups, share, 2, QK_DIM)

    def scores(eq, n, lo):
        keys = (cache if n else fresh)[..., lo * QK_DIM : (lo + 1) * QK_DIM]
        return jnp.einsum(eq, grouped[:, :, :, lo], keys, preferred_element_type=F32) * scale

    first = scores("bgjd,bgkd->bgjk", 1, 0)
    second = scores("bgjd,bgkd->bgjk", 1, 1)
    first_new = scores("bgjd,bgd->bgj", 0, 0)
    second_new = scores("bgjd,bgd->bgj", 0, 1)
    valid = (
        jnp.arange(cache.shape[2], dtype=jnp.int32)[None, None, None, :]
        < lengths[:, None, None, None]
    )
    prob_one, prob_one_new = normalize(first, first_new, valid)
    prob_two, prob_two_new = normalize(second, second_new, valid)
    weight = lam.reshape(groups, share)[None, :, :, None]
    mapped = (prob_one - weight * prob_two).astype(BF16)
    mapped_new = (prob_one_new - weight[..., 0] * prob_two_new).astype(BF16)
    output = jnp.einsum(
        "bgjk,bgkd->bgjd", mapped, cache[..., 2 * QK_DIM :], preferred_element_type=F32
    )
    output = output + mapped_new.astype(F32)[..., None] * fresh[:, :, None, 2 * QK_DIM :].astype(F32)
    return output.reshape(count, groups * share, HEAD_DIM)


def dot(a, b):
    return jnp.dot(a, b, preferred_element_type=F32)


def up(v, n, size):
    return lax.rem(v + (n % size), size)


def tail_kernel(
    heads, resid, gain, mix_w, ids_t, rw_t, wo_h, eg_h, eu_h, ed_h, dg_h, du_h, dd_h, out,
    wo, we, wd, ed, dd, edx, hg, sg, xg, he, hd, st, wc, mc, hx, slots, eo,
    s0, r0, own, s1, r1, bsum, s2, r2,
    lsem, ed_s, ed_r, h_s, h_r, c_s, c_r, g_s, g_r, x_s, x_r, s0_s, s0_r, s1_s, s1_r, s2_s, s2_r,
):
    e = lax.axis_index("ep")
    t = lax.axis_index("tp")
    z = lax.div(e, 8)
    x = lax.rem(lax.div(e, 2), 4)
    c = lax.rem(e, 2)

    def dev(dz=0, dx=0, flip=False, dy=0):
        cc = 1 - c if flip else c
        return {
            "ep": (up(z, dz, NZ) * NX + up(x, dx, NX)) * NC + cc,
            "tp": up(t, dy, NY),
        }

    def remote(src, dst, ssem, rsem, to):
        return pltpu.make_async_remote_copy(
            src_ref=src, dst_ref=dst, send_sem=ssem, recv_sem=rsem, device_id=to, device_id_type=MESH
        )

    loads = [
        pltpu.make_async_copy(ed_h, ed, lsem.at[0]),
        pltpu.make_async_copy(wo_h, wo, lsem.at[1]),
        pltpu.make_async_copy(eg_h, we.at[:, pl.ds(0, FF)], lsem.at[2]),
        pltpu.make_async_copy(eu_h, we.at[:, pl.ds(FF, FF)], lsem.at[3]),
        pltpu.make_async_copy(dg_h, wd.at[:, pl.ds(0, FF)], lsem.at[4]),
        pltpu.make_async_copy(du_h, wd.at[:, pl.ds(FF, FF)], lsem.at[5]),
        pltpu.make_async_copy(dd_h.at[:, pl.ds(pl.multiple_of(t * Q, Q), Q)], dd, lsem.at[6]),
    ]
    for load in loads:
        load.start()

    barrier = pltpu.get_barrier_semaphore()
    peers = (
        [dev(dy=k) for k in (1, 2, 3)]
        + [dev(dx=k) for k in (1, 2, 3)]
        + [dev(dz=k) for k in range(1, 8)]
        + [dev(flip=True)]
    )
    for peer in peers:
        pl.semaphore_signal(barrier, inc=1, device_id=peer, device_id_type=MESH)

    ids_f = ids_t[...].astype(F32)
    rw = rw_t[...]
    row16 = lax.broadcasted_iota(jnp.int32, (SEQ, SEQ), 0)
    col16 = lax.broadcasted_iota(jnp.int32, (SEQ, SEQ), 1)
    eye = row16 == col16

    def column(rows, k):
        spread = jnp.broadcast_to(rows[k : k + 1, :], (SEQ, SEQ))
        return jnp.sum(jnp.where(eye, spread, 0.0), axis=1, keepdims=True)

    lane = lax.broadcasted_iota(jnp.int32, (SEQ, INFO), 1)
    lane_f = lane.astype(F32)
    id_cols = [column(ids_f, k) for k in (0, 1)]
    w_cols = [column(rw, k) for k in (0, 1)]
    member = jnp.where(lane_f == id_cols[0], 1.0, 0.0) + jnp.where(lane_f == id_cols[1], 1.0, 0.0)
    before = jnp.where(row16 > col16, 1.0, 0.0).astype(BF16)
    earlier = dot(before, member.astype(BF16))

    def split3(v):
        hi = v.astype(BF16).astype(F32)
        rest = v - hi
        mid = rest.astype(BF16).astype(F32)
        return [hi, mid, rest - mid]

    fields = list(id_cols)
    for k in (0, 1):
        fields.append(
            jnp.sum(jnp.where(lane_f == id_cols[k], earlier, 0.0), axis=1, keepdims=True)
        )
    fields += split3(w_cols[0]) + split3(w_cols[1])
    info = jnp.zeros((SEQ, INFO), F32)
    for i, field in enumerate(fields):
        info = jnp.where(lane == i, field, info)

    pl.semaphore_wait(barrier, 14)

    heads_out = [
        remote(heads, hg.at[t], h_s.at[k - 1], h_r.at[k - 1], dev(dy=k)) for k in (1, 2, 3)
    ]
    for copy in heads_out:
        copy.start()
    loads[0].wait()
    ed_out = []
    for k in (1, 2, 3):
        cols = pl.ds(pl.multiple_of(up(t, k, NY) * Q, Q), Q)
        copy = remote(ed.at[:, cols], edx.at[t], ed_s.at[k - 1], ed_r.at[k - 1], dev(dy=k))
        copy.start()
        ed_out.append(copy)
    own_cols = pl.ds(pl.multiple_of(t * Q, Q), Q)
    loads[1].wait()

    def wo_rows(src):
        return wo[pl.ds(pl.multiple_of(src * Q, Q), Q), :]

    total = resid[:, own_cols].astype(F32) + dot(heads[...], wo_rows(t))
    for k in (1, 3, 2):
        src = up(t, -k, NY)
        remote(heads, hg.at[src], h_s.at[k - 1], h_r.at[k - 1], dev()).wait_recv()
        total = total + dot(hg[src], wo_rows(src))
    stream_cols = total.astype(BF16)
    sg[t] = stream_cols
    cols_out = [
        remote(sg.at[t], sg.at[t], c_s.at[k - 1], c_r.at[k - 1], dev(dy=k)) for k in (1, 2, 3)
    ]
    for copy in cols_out:
        copy.start()
    for k in (1, 3, 2):
        src = up(t, -k, NY)
        remote(sg.at[src], sg.at[src], c_s.at[k - 1], c_r.at[k - 1], dev()).wait_recv()
    stream = jnp.concatenate([sg[k] for k in range(NY)], axis=1).astype(F32)
    ffn_in = rms_rows(stream, gain[...]).astype(BF16)
    mix = jax.nn.sigmoid(jnp.sum(ffn_in.astype(F32) * mix_w[...], axis=-1, keepdims=True))
    for i, field in enumerate(split3(mix)):
        info = jnp.where(lane == 10 + i, field, info)
    xg[x, c, z, :, 0:D] = ffn_in
    xg[x, c, z, :, D:WIDE] = info.astype(BF16)

    counter = [0]

    def send(px, pc, pz, **to):
        i = counter[0]
        counter[0] += 1
        remote(xg.at[px, pc, pz], xg.at[px, pc, pz], g_s.at[i], g_r.at[px, pc, pz], dev(**to)).start()

    def arrive(px, pc, pz):
        ref = xg.at[px, pc, pz]
        remote(ref, ref, g_s.at[0], g_r.at[px, pc, pz], dev()).wait_recv()

    @pl.when(c == 0)
    def _():
        counter[0] = 0
        for k in (1, 3, 2):
            send(x, 0, z, dx=k)
        send(x, 0, z, dz=1)
        send(x, 0, z, dz=-1)
        send(x, 0, z, flip=True)
        for k in (1, 3, 2):
            px = up(x, k, NX)
            arrive(px, 0, z)
            send(px, 0, z, dz=1)
            send(px, 0, z, dz=-1)
            send(px, 0, z, flip=True)
        for step in (1, 2, 3):
            for j, k in enumerate(X_ORDER):
                px = up(x, k, NX)
                for sign in (1, -1):
                    pz = up(z, -sign * step, NZ)
                    arrive(px, 0, pz)
                    if step < 3 or (j < 2) == (sign == 1):
                        send(px, 0, pz, dz=sign)
                    send(px, 0, pz, flip=True)
        for k in X_ORDER:
            px = up(x, k, NX)
            pz = up(z, 4, NZ)
            arrive(px, 0, pz)
            send(px, 0, pz, flip=True)
        assert counter[0] == N_SENDS

    @pl.when(c == 1)
    def _():
        counter[0] = 0
        z_order = [0, -1, 1, -2, 2, -3, 3, 4]
        for m, k in enumerate(z_order):
            pz = up(z, k, NZ)
            if m:
                arrive(x, 1, pz)
            if m == 0:
                send(x, 1, pz, dz=1)
                send(x, 1, pz, dz=-1)
            elif k < 0:
                send(x, 1, pz, dz=1)
            elif k < 3:
                send(x, 1, pz, dz=-1)
            send(x, 1, pz, dx=1)
            send(x, 1, pz, dx=-1)
            send(x, 1, pz, flip=True)
        for m, k in enumerate(z_order):
            pz = up(z, k, NZ)
            for sign in (1, -1):
                px = up(x, -sign, NX)
                arrive(px, 1, pz)
                if (m % 2 == 0) == (sign == 1):
                    send(px, 1, pz, dx=sign)
                send(px, 1, pz, flip=True)
        for k in z_order:
            px = up(x, 2, NX)
            pz = up(z, k, NZ)
            arrive(px, 1, pz)
            send(px, 1, pz, flip=True)
        assert counter[0] == N_SENDS

    def sibling_arrival(i, carry):
        arrive(lax.div(i, NZ), 1 - c, lax.rem(i, NZ))
        return carry

    lax.fori_loop(0, NX * NZ, sibling_arrival, 0)

    for load in loads[2:]:
        load.wait()
    e_f = e.astype(F32)
    brow = lax.broadcasted_iota(jnp.int32, (INFO, INFO), 0)
    spans = ((0, 1), (1, 2), (2, 3), (3, 4), (4, 7), (7, 10), (10, 13))
    spread = jnp.concatenate(
        [jnp.where((brow >= lo) & (brow < hi), 1.0, 0.0).astype(BF16) for lo, hi in spans], axis=1
    )
    rows = NC * NZ * SEQ
    rr = lax.broadcasted_iota(jnp.int32, (rows, INFO), 0)
    ll = lax.broadcasted_iota(jnp.int32, (rows, INFO), 1)
    rel = (ll - 2 * lax.div(rr, SEQ)).astype(F32)

    def expert_rows(i, carry):
        block = xg[i].reshape(rows, WIDE)
        both = dot(block[:, 0:D], we[...])
        hidden = (jax.nn.silu(both[:, 0:FF]) * both[:, FF:]).astype(BF16)
        b = dot(block[:, D:WIDE], spread)
        part = [b[:, k * INFO : (k + 1) * INFO] for k in range(7)]
        m0 = part[0] == e_f
        m1 = part[1] == e_f
        wc[i] = jnp.where(m0, part[4], 0.0) + jnp.where(m1, part[5], 0.0)
        mc[i] = part[6]
        slot = jnp.where(m0, part[2], jnp.where(m1, part[3], -4096.0))
        base = (i * (2 * NC * NZ)).astype(F32)
        chosen = jnp.where(slot == rel - base, 1.0, 0.0).astype(BF16)
        st[i] = chosen
        he[...] = hidden
        got = lax.dot_general(
            st[i], he[...], (((0,), (0,)), ((), ())), preferred_element_type=F32
        )

        @pl.when(i == 0)
        def _():
            slots[...] = got

        @pl.when(i > 0)
        def _():
            slots[...] += got

        return carry

    lax.fori_loop(0, NX, expert_rows, 0)
    hx[t] = slots[...].astype(BF16)
    hid_out = [
        remote(hx.at[t], hx.at[t], x_s.at[k - 1], x_r.at[k - 1], dev(dy=k)) for k in (1, 2, 3)
    ]
    for copy in hid_out:
        copy.start()

    def dense_rows(i, carry):
        block = xg[i].reshape(rows, WIDE)
        both = dot(block[:, 0:D], wd[...])
        hd[i] = (jax.nn.silu(both[:, 0:FF]) * both[:, FF:]).astype(BF16)
        return carry

    lax.fori_loop(0, NX, dense_rows, 0)

    edx[t] = ed[:, own_cols]
    for k in (1, 3, 2):
        src = up(t, -k, NY)
        remote(edx.at[src], edx.at[src], ed_s.at[k - 1], ed_r.at[k - 1], dev()).wait_recv()
        remote(hx.at[src], hx.at[src], x_s.at[k - 1], x_r.at[k - 1], dev()).wait_recv()
    result = jnp.zeros((2 * NX * NC * NZ, Q), F32)
    for k in range(NY):
        result = result + dot(hx[k], edx[k]).astype(BF16).astype(F32)
    eo[...] = result.astype(BF16)

    half = NZ * SEQ

    def part_of(px, pc):
        at = pl.ds(pl.multiple_of(pc * half, half), half)
        four = lambda a: jnp.concatenate([a] * 4, axis=1)
        dense = dot(hd[px, at, :], dd[...])
        routed = dot(st[px, at, :], eo[...])
        return four(mc[px, at, :]) * dense + four(wc[px, at, :]) * routed

    x_seq = (2, 1, 3, 0)
    pair_out = {}
    for k in x_seq:
        px = up(x, k, NX)
        s0[k] = part_of(px, 1 - c).astype(BF16)
        pair_out[k] = remote(s0.at[k], r0.at[k], s0_s.at[k], s0_r.at[k], dev(flip=True))
        pair_out[k].start()
        own[k] = part_of(px, c)
    x_out = {}
    for k in x_seq:
        pair_out[k].wait_recv()
        joined = own[k] + r0[k].astype(F32)
        if k:
            s1[k - 1] = joined.astype(BF16)
            x_out[k] = remote(s1.at[k - 1], r1.at[k - 1], s1_s.at[k - 1], s1_r.at[k - 1], dev(dx=k))
            x_out[k].start()
        else:
            own[0] = joined
    sums = own[0]
    for k in (1, 3, 2):
        x_out[k].wait_recv()
        sums = sums + r1[k - 1].astype(F32)
    bsum[...] = sums.reshape(NZ, SEQ, Q)
    s2[...] = sums.astype(BF16).reshape(NZ, SEQ, Q)
    z_out = []
    for k in (4, 3, 5, 2, 6, 1, 7):
        pz = up(z, k, NZ)
        copy = remote(s2.at[pz], r2.at[k - 1], s2_s.at[k - 1], s2_r.at[k - 1], dev(dz=k))
        copy.start()
        z_out.append(copy)
    final = stream_cols.astype(F32) + bsum[z]
    for copy in reversed(z_out):
        copy.wait_recv()
    for k in range(NZ - 1):
        final = final + r2[k].astype(F32)
    out[...] = final

    for copy in heads_out + ed_out + cols_out + hid_out + list(pair_out.values()):
        copy.wait_send()
    for copy in list(x_out.values()) + z_out:
        copy.wait_send()

    def sent(i, carry):
        ref = xg.at[0, 0, 0]
        remote(ref, ref, g_s.at[i], g_r.at[0, 0, 0], dev()).wait_send()
        return carry

    lax.fori_loop(0, N_SENDS, sent, 0)


def tail(*operands):
    vmem = pl.BlockSpec(memory_space=pltpu.VMEM)
    hbm = pl.BlockSpec(memory_space=pl.ANY)
    rows = NC * NZ * SEQ
    dma = lambda *n: pltpu.SemaphoreType.DMA(n)
    buf = lambda shape, kind=BF16: pltpu.VMEM(shape, kind)
    return pl.pallas_call(
        tail_kernel,
        out_shape=jax.ShapeDtypeStruct((SEQ, Q), F32),
        in_specs=[vmem] * 6 + [hbm] * 7,
        out_specs=vmem,
        scratch_shapes=[
            buf((D, Q)),
            buf((D, 2 * FF)),
            buf((D, 2 * FF)),
            buf((FF, D)),
            buf((FF, Q)),
            buf((NY, FF, Q)),
            buf((NY, SEQ, Q)),
            buf((NY, SEQ, Q)),
            buf((NX, NC, NZ, SEQ, WIDE)),
            buf((rows, FF)),
            buf((NX, rows, FF)),
            buf((NX, rows, INFO)),
            buf((NX, rows, INFO), F32),
            buf((NX, rows, INFO), F32),
            buf((NY, 128, FF)),
            buf((128, FF), F32),
            buf((128, Q)),
            buf((NX, NZ * SEQ, Q)),
            buf((NX, NZ * SEQ, Q)),
            buf((NX, NZ * SEQ, Q), F32),
            buf((NX - 1, NZ * SEQ, Q)),
            buf((NX - 1, NZ * SEQ, Q)),
            buf((NZ, SEQ, Q), F32),
            buf((NZ, SEQ, Q)),
            buf((NZ - 1, SEQ, Q)),
            dma(7),
            dma(3), dma(3), dma(3), dma(3), dma(3), dma(3),
            dma(N_SENDS), dma(NX, NC, NZ),
            dma(3), dma(3), dma(4), dma(4), dma(3), dma(3), dma(7), dma(7),
        ],
        compiler_params=pltpu.CompilerParams(
            collective_id=0, has_side_effects=True, vmem_limit_bytes=48 * 1024 * 1024
        ),
        name="tail",
    )(*operands)


def on_device(
    residual_in, lengths, kv_cache, norm_gain_attn, query_weight, key_weight, value_weight,
    diff_lambda, head_gain, out_weight, norm_gain_ffn, route_ids, route_weights, expert_gate,
    expert_up, expert_down, dense_gate, dense_up, dense_down, dense_mix,
):
    seq_count, width = residual_in.shape
    groups = kv_cache.shape[1]
    local_heads = diff_lambda.shape[0]
    resid = residual_in.astype(F32)
    normed = rms_rows(resid, norm_gain_attn).astype(BF16)
    positions = lengths.astype(F32)
    query = dot(normed, query_weight).reshape(seq_count, local_heads, 2, QK_DIM)
    query = rotate(query, positions).astype(BF16)
    keys = dot(normed, key_weight).reshape(seq_count, groups, 2, QK_DIM)
    keys = rotate(keys, positions).astype(BF16).reshape(seq_count, groups, 2 * QK_DIM)
    values = dot(normed, value_weight).reshape(seq_count, groups, HEAD_DIM).astype(BF16)
    fresh = jnp.concatenate([keys, values], axis=-1)
    mixed = attend(query, fresh, kv_cache, lengths, diff_lambda)
    heads_out = rms_rows(mixed, head_gain).astype(BF16).reshape(seq_count, local_heads * HEAD_DIM)
    final = tail(
        heads_out,
        residual_in,
        norm_gain_ffn.reshape(1, width),
        dense_mix.reshape(1, width),
        route_ids.T,
        route_weights.T,
        out_weight,
        expert_gate.reshape(width, -1),
        expert_up.reshape(width, -1),
        expert_down.reshape(-1, width),
        dense_gate,
        dense_up,
        dense_down,
    )
    return (final.astype(BF16), fresh)


def solution(mesh):
    placed = (
        P("ep", None),
        P("ep"),
        P("ep", "tp", None, None),
        P(),
        P(None, "tp"),
        P(None, "tp"),
        P(None, "tp"),
        P("tp"),
        P(),
        P(None, "tp"),
        P(),
        P("ep", None),
        P("ep", None),
        P("ep", None, "tp"),
        P("ep", None, "tp"),
        P("ep", "tp", None),
        P(None, "ep"),
        P(None, "ep"),
        P("ep", None),
        P(),
    )
    return jax.shard_map(
        on_device,
        mesh=mesh,
        in_specs=placed,
        out_specs=(P("ep", "tp"), P("ep", "tp", None)),
        check_vma=False,
    )
```

time: 178 us -> 80.9 us (0.45)
  Pallas kernels: 0 us -> 65.8 us
  waiting for transfers between devices: 56.8 us -> 0 us
  blocking collectives: 52.3 us -> 0 us
  starting transfers between devices: 18 us -> 0 us
  matrix products: 24.6 us -> 9.09 us
  between operations: 14.3 us -> 0.95 us
  local copies, waits for them, and re-layouts: 4.77 us -> 1.45 us
  other arithmetic: 6.57 us -> 3.33 us
    pallas_call x0 -> x1, Pallas kernels: none -> 65.8 us  [tail(): pl.pallas_call(tail_kernel, out_shape=jax.ShapeDtypeStruct((SEQ, Q), F32)...]
    all_to_all x3 -> x0, blocking collectives: 52.3 us -> none  [the longest x1 33.7 us: on_device(): lax.all_to_all(outgoing, 'ep', split_axis=0, concat_axis=0, tiled=True)]
    all_to_all x3 -> x0, waiting for transfers between devices: 30.6 us -> none  [the longest x1 26.1 us: summed_on_arrival(): lax.all_to_all(pieces, axis, split_axis=0, concat_axis=0, tiled=True)]
    all_gather x1 -> x0, waiting for transfers between devices: 26.2 us -> none  [on_device(): piece = lax.all_gather(ffn_in, 'ep', axis=0, tiled=True)]
    all_to_all x3 -> x0, starting transfers between devices: 18 us -> none  [the longest x1 6.69 us: summed_on_arrival(): lax.all_to_all(pieces, axis, split_axis=0, concat_axis=0, tiled=True)]
    dot_general x13 -> x7, matrix products: 24.1 us -> 6.78 us  [the longest x4 5.06 us: scores(): jnp.einsum(eq, grouped[:, :, :, lo], keys, preferred_element_type=F32)]
  transfers between devices with their start and end apart: 4 -> 0, of which waited for: 3 -> 0; matrix products, arithmetic and copies ran while one was open for 10% -> 0% of each run, Pallas kernels for 0% -> 0%
where the time goes in v1:
time: 80.9 us; the launch traced here: 80.6 us
  Pallas kernels  65.8 us (81%)
  matrix products  9.09 us (11%)
  other arithmetic  3.33 us (4%)
  local copies, waits for them, and re-layouts  1.45 us (2%)
  between operations  0.95 us (1%)
    pallas_call x1, Pallas kernels, tail(): pl.pallas_call(tail_kernel, out_shape=jax.ShapeDtypeStruct((SEQ, Q), F32)...  65.8 us
    dot_general x4, matrix products, scores(): jnp.einsum(eq, grouped[:, :, :, lo], keys, preferred_element_type=F32)  5.06 us
    dot_general x1, matrix products, attend(): jnp.einsum('bgjk,bgkd->bgjd', mapped, cache[..., 2 * QK_DIM:], preferred_...  2.3 us
    dot_general x3, matrix products, dot(): return jnp.dot(a, b, preferred_element_type=F32)  1.73 us

profile of v1, /device:TPU:1, one launch (start us, length us, event | category | flops | bytes accessed | tf_op | source)
XLA Modules:
  0.0 80.6 jit_solution(7291962956736815676)
XLA Ops:
  0.6 0.0 copy-start
  0.7 1.1 %fusion.14 = f32[16]{0:T(128)S(1)} fusion(bf16[16,2048]{1,0:T(8,128)(2,1)} %resid.1), kind=kLoop, calls=%fused_computation.15 | loop fusion | flops 98288 | bytes 65600 | tf_op jit(solution)/shard_map/reduce_sum | solution.py:26
  1.8 0.5 copy-done
  2.3 1.3 %fusion.45 = f32[16,512]{1,0:T(8,128)S(1)} fusion(bf16[2048,512]{1,0:T(8,128)(2,1)S(1)} %copy-done, bf16[16,2048]{1,0:T(8,128)(2,1)} %resid.1, f32[2048]{0:T(1024)} %param.23, f32[16]{0:T(128)S(1)} %add_rsqrt_fusion.1), kind=kOutput, calls=%fused_computation.73 | convolution fusion | flops 33685504 | bytes 2203712 | tf_op jit(solution)/shard_map/dot_general | solution.py:84
  3.5 0.1 reshape.293
  3.6 0.1 fusion.47
  3.8 0.1 multiply_cosine_fusion
  4.0 0.1 fusion.33
  4.1 0.0 copy-start.2
  4.1 2.4 %fusion.10 = f32[16,4,512]{2,1,0:T(4,128)S(1)} fusion(bf16[16,4,64]{2,1,0:T(4,128)(2,1)S(1)} %get-tuple-element.8, bf16[16,1,512,256]{3,2,1,0:T(8,128)(2,1)} %param.22), kind=kOutput, calls=%fused_computation.9 | convolution fusion | flops 4227072 | bytes 2236416 | tf_op jit(solution)/shard_map/bgjd,bgkd->bgjk/dot_general | solution.py:61
  6.5 0.1 iota_compare_fusion
  6.6 2.4 %select_reduce_fusion.1 = (f32[16,4]{1,0:T(8,128)S(1)}, f32[16,4]{1,0:T(8,128)S(1)}, f32[16,4,512]{2,1,0:T(4,128)S(1)}) fusion(pred[16,512]{1,0:T(8,128)(4,1)S(1)} %iota_compare_fusion, f32[16,4,512]{2,1,0:T(4,128)S(1)} %fusion.10, bf16[16,4,64]{2,1,0:T(4,128)(2,1)S(1)} %get-tuple-element.9, bf16[16,1,512,256]{3,2,1,0:T(8,128)(2,1)} %param.22), kind=kOutput, calls=%fused_computation.21 | convolution fusion | flops 4358016 | bytes 2376192 | tf_op jit(solution)/shard_map/bgjd,bgkd->bgjk/dot_general | solution.py:61
  9.0 0.0 copy-done.15
  9.0 0.2 fusion.43
  9.2 0.1 reshape.296
  9.3 0.1 subtract_convert_fusion.1
  9.4 0.1 pad_maximum_fusion.1
  9.5 0.1 convert_element_type.64
  9.6 0.1 slice_bitcast_fusion.4
  9.7 0.1 fusion.34
  9.8 0.1 fusion.36
  10.0 0.3 fusion.18
  10.3 0.2 fusion.48
  10.6 0.0 copy-start.3
  10.7 2.3 %multiply_reduce_fusion = (f32[16,4]{1,0:T(8,128)S(1)}, f32[16,4,128]{2,1,0:T(4,128)S(1)}) fusion(f32[16,128]{1,0:T(8,128)S(1)} %get-tuple-element.22, f32[16,4]{1,0:T(8,128)S(1)} %get-tuple-element.14, bf16[16,1,512,256]{3,2,0,1:T(8,128)(2,1)} %bitcast.71, f32[16,4,512]{2,1,0:T(4,128)S(1)} %get-tuple-element.21, f32[16,4,512]{2,1,0:T(4,128)S(1)} %fusion.10, ...), kind=kOutput, calls=%fused_computation.38 | convolution fusion | flops 8781760 | bytes 2410000 | tf_op jit(solution)/shard_map/bgjk,bgkd->bgjd/dot_general | solution.py:76
  13.0 0.1 broadcast_multiply_fusion
  13.2 0.1 copy-done.5
  13.3 0.2 copy-done.6
  13.4 0.2 copy-done.7
  13.6 65.8 %tail.1 = f32[16,512]{1,0:T(8,128)S(1)} custom-call(bf16[16,512]{1,0:T(8,128)(2,1)S(1)} %fusion.28.heads, bf16[16,2048]{1,0:T(8,128)(2,1)S(1)} %copy-done.2, f32[1,2048]{1,0:T(1,128)S(1)} %bitcast.67, f32[1,2048]{1,0:T(1,128)S(1)} %bitcast.68, s32[2,16]{1,0:T(2,128)S(1)} %bitcast.69, f32[2,16]{1,0:T(2,128)S(1)} %bitcast.70, bf16[2048,512]{1,0:T(8,128)(2,1)S(1)} %copy-done.1, ...), custom_call_target="tpu_custom_call" | custom-call | tf_op jit(solution)/shard_map/tail/pallas_call | solution.py:427
  79.4 0.6 convert_element_type.71
  80.0 0.6 pad_maximum_fusion.2
  (39 shorter events, 0.2 us)
Async XLA Ops:
  0.6 1.6 %copy-start = (bf16[2048,512]{1,0:T(8,128)(2,1)S(1)}, bf16[2048,512]{1,0:T(8,128)(2,1)}, u32[]{:S(2)}) copy-start(bf16[2048,512]{1,0:T(8,128)(2,1)} %param.24) | copy-start | bytes 6291460
  0.6 3.1 %copy-start.17 = (s32[16]{0:T(128)S(1)}, s32[16]{0:T(128)}, u32[]{:S(2)}) copy-start(s32[16]{0:T(128)} %param.21) | copy-start | bytes 196
  4.1 4.9 %copy-start.2 = (bf16[16,2048]{1,0:T(8,128)(2,1)S(1)}, bf16[16,2048]{1,0:T(8,128)(2,1)}, u32[]{:S(2)}) copy-start(bf16[16,2048]{1,0:T(8,128)(2,1)} %resid.1) | copy-start | bytes 196612
  4.1 4.9 %copy-start.13 = (bf16[2048,128]{1,0:T(8,128)(2,1)S(1)}, bf16[2048,128]{1,0:T(8,128)(2,1)}, u32[]{:S(2)}) copy-start(bf16[2048,128]{1,0:T(8,128)(2,1)} %param.25) | copy-start | bytes 1572868
  4.1 4.9 %copy-start.15 = (f32[2048]{0:T(1024)S(1)}, f32[2048]{0:T(1024)}, u32[]{:S(2)}) copy-start(f32[2048]{0:T(1024)} %param.23) | copy-start | bytes 24580
  6.5 3.8 %copy-start.16 = (f32[4]{0:T(128)S(1)}, f32[4]{0:T(128)}, u32[]{:S(2)}) copy-start(f32[4]{0:T(128)} %param.27) | copy-start | bytes 52
  6.5 3.8 %copy-start.14 = (bf16[2048,128]{1,0:T(8,128)(2,1)S(1)}, bf16[2048,128]{1,0:T(8,128)(2,1)}, u32[]{:S(2)}) copy-start(bf16[2048,128]{1,0:T(8,128)(2,1)} %param.26) | copy-start | bytes 1572868
  10.3 2.8 %copy-start.8 = (bf16[128,2048]{1,0:T(8,128)(2,1)S(1)}, bf16[128,2048]{1,0:T(8,128)(2,1)}, u32[]{:S(2)}) copy-start(bf16[128,2048]{1,0:T(8,128)(2,1)} %dd_h.1) | copy-start | bytes 1572868
  10.6 2.5 %copy-start.18 = (f32[128]{0:T(128)S(1)}, f32[128]{0:T(128)}, u32[]{:S(2)}) copy-start(f32[128]{0:T(128)} %param.28) | copy-start | bytes 1540
  10.6 2.6 %copy-start.1 = (bf16[2048,512]{1,0:T(8,128)(2,1)S(1)}, bf16[2048,512]{1,0:T(8,128)(2,1)}, u32[]{:S(2)}) copy-start(bf16[2048,512]{1,0:T(8,128)(2,1)} %wo_h.1) | copy-start | bytes 6291460
  10.6 2.6 %copy-start.3 = (bf16[1,2048,128]{2,1,0:T(8,128)(2,1)S(1)}, bf16[1,2048,128]{2,1,0:T(8,128)(2,1)}, u32[]{:S(2)}) copy-start(bf16[1,2048,128]{2,1,0:T(8,128)(2,1)} %param.33) | copy-start | bytes 1572868
  10.6 2.6 %copy-start.4 = (bf16[1,2048,128]{2,1,0:T(8,128)(2,1)S(1)}, bf16[1,2048,128]{2,1,0:T(8,128)(2,1)}, u32[]{:S(2)}) copy-start(bf16[1,2048,128]{2,1,0:T(8,128)(2,1)} %param.34) | copy-start | bytes 1572868
  10.6 2.6 %copy-start.5 = (bf16[1,128,2048]{2,1,0:T(8,128)(2,1)S(1)}, bf16[1,128,2048]{2,1,0:T(8,128)(2,1)}, u32[]{:S(2)}) copy-start(bf16[1,128,2048]{2,1,0:T(8,128)(2,1)} %param.35) | copy-start | bytes 1572868
  10.6 2.8 %copy-start.6 = (bf16[2048,128]{1,0:T(8,128)(2,1)S(1)}, bf16[2048,128]{1,0:T(8,128)(2,1)}, u32[]{:S(2)}) copy-start(bf16[2048,128]{1,0:T(8,128)(2,1)} %dg_h.1) | copy-start | bytes 1572868
  10.7 2.9 %copy-start.7 = (bf16[2048,128]{1,0:T(8,128)(2,1)S(1)}, bf16[2048,128]{1,0:T(8,128)(2,1)}, u32[]{:S(2)}) copy-start(bf16[2048,128]{1,0:T(8,128)(2,1)} %du_h.1) | copy-start | bytes 1572868
  10.7 2.9 %copy-start.9 = (f32[2048]{0:T(1024)S(1)}, f32[2048]{0:T(1024)}, u32[]{:S(2)}) copy-start(f32[2048]{0:T(1024)} %param.30) | copy-start | bytes 24580
  10.7 2.9 %copy-start.10 = (f32[2048]{0:T(1024)S(1)}, f32[2048]{0:T(1024)}, u32[]{:S(2)}) copy-start(f32[2048]{0:T(1024)} %param.39) | copy-start | bytes 24580
  10.7 2.9 %copy-start.11 = (s32[16,2]{0,1:T(2,128)S(1)}, s32[16,2]{0,1:T(2,128)}, u32[]{:S(2)}) copy-start(s32[16,2]{0,1:T(2,128)} %param.31) | copy-start | bytes 388
  10.7 2.9 %copy-start.12 = (f32[16,2]{0,1:T(2,128)S(1)}, f32[16,2]{0,1:T(2,128)}, u32[]{:S(2)}) copy-start(f32[16,2]{0,1:T(2,128)} %param.32) | copy-start | bytes 388

commit v2 on v1

--- a/solution.py
+++ b/solution.py
@@ -1,5 +1,6 @@
 import jax
 import jax.numpy as jnp
+import numpy as np
 from jax import lax
 from jax.experimental import pallas as pl
 from jax.experimental.pallas import tpu as pltpu
@@ -27,59 +28,6 @@
     return values * lax.rsqrt(mean_sq + EPS) * gain
 
 
-def rotate(vectors, positions):
-    half = vectors.shape[-1] // 2
-    inverse = 10000.0 ** (-jnp.arange(half, dtype=jnp.float32) / half)
-    angle = positions[:, None, None, None] * inverse
-    cosine = jnp.cos(angle)
-    sine = jnp.sin(angle)
-    first = vectors[..., :half]
-    second = vectors[..., half:]
-    return jnp.concatenate(
-        [first * cosine - second * sine, first * sine + second * cosine], axis=-1
-    )
-
-
-def normalize(scores, latest, valid):
-    masked = jnp.where(valid, scores, -jnp.inf)
-    top = jnp.maximum(jnp.max(masked, axis=-1), latest)
-    raised = jnp.where(valid, jnp.exp(jnp.where(valid, scores, 0.0) - top[..., None]), 0.0)
-    raised_new = jnp.exp(latest - top)
-    total = jnp.sum(raised, axis=-1) + raised_new
-    return (raised / total[..., None], raised_new / total)
-
-
-def attend(query, fresh, cache, lengths, lam):
-    count = fresh.shape[0]
-    groups = fresh.shape[1]
-    share = query.shape[1] // groups
-    scale = QK_DIM ** (-0.5)
-    grouped = query.reshape(count, groups, share, 2, QK_DIM)
-
-    def scores(eq, n, lo):
-        keys = (cache if n else fresh)[..., lo * QK_DIM : (lo + 1) * QK_DIM]
-        return jnp.einsum(eq, grouped[:, :, :, lo], keys, preferred_element_type=F32) * scale
-
-    first = scores("bgjd,bgkd->bgjk", 1, 0)
-    second = scores("bgjd,bgkd->bgjk", 1, 1)
-    first_new = scores("bgjd,bgd->bgj", 0, 0)
-    second_new = scores("bgjd,bgd->bgj", 0, 1)
-    valid = (
-        jnp.arange(cache.shape[2], dtype=jnp.int32)[None, None, None, :]
-        < lengths[:, None, None, None]
-    )
-    prob_one, prob_one_new = normalize(first, first_new, valid)
-    prob_two, prob_two_new = normalize(second, second_new, valid)
-    weight = lam.reshape(groups, share)[None, :, :, None]
-    mapped = (prob_one - weight * prob_two).astype(BF16)
-    mapped_new = (prob_one_new - weight[..., 0] * prob_two_new).astype(BF16)
-    output = jnp.einsum(
-        "bgjk,bgkd->bgjd", mapped, cache[..., 2 * QK_DIM :], preferred_element_type=F32
-    )
-    output = output + mapped_new.astype(F32)[..., None] * fresh[:, :, None, 2 * QK_DIM :].astype(F32)
-    return output.reshape(count, groups * share, HEAD_DIM)
-
-
 def dot(a, b):
     return jnp.dot(a, b, preferred_element_type=F32)
 
@@ -88,8 +36,11 @@
     return lax.rem(v + (n % size), size)
 
 
-def tail_kernel(
-    heads, resid, gain, mix_w, ids_t, rw_t, wo_h, eg_h, eu_h, ed_h, dg_h, du_h, dd_h, out,
+def layer_kernel(
+    resid_h, lens_h, kv_h, ga_h, wq_h, wk_h, wv_h, lam_h, hgain_h, wo_h, gf_h, ids_h, rw_h,
+    eg_h, eu_h, ed_h, dg_h, du_h, dd_h, mixw_h, inv_h, out, rows_out,
+    resid, lens, kv, gain_a, wqkv, lam, hgain, gain, ids_t, rw_t, mix_w, inv,
+    qs, fk, fv, lenb, mixed, heads,
     wo, we, wd, ed, dd, edx, hg, sg, xg, he, hd, st, wc, mc, hx, slots, eo,
     s0, r0, own, s1, r1, bsum, s2, r2,
     lsem, ed_s, ed_r, h_s, h_r, c_s, c_r, g_s, g_r, x_s, x_r, s0_s, s0_r, s1_s, s1_r, s2_s, s2_r,
@@ -112,17 +63,25 @@
             src_ref=src, dst_ref=dst, send_sem=ssem, recv_sem=rsem, device_id=to, device_id_type=MESH
         )
 
-    loads = [
-        pltpu.make_async_copy(ed_h, ed, lsem.at[0]),
-        pltpu.make_async_copy(wo_h, wo, lsem.at[1]),
-        pltpu.make_async_copy(eg_h, we.at[:, pl.ds(0, FF)], lsem.at[2]),
-        pltpu.make_async_copy(eu_h, we.at[:, pl.ds(FF, FF)], lsem.at[3]),
-        pltpu.make_async_copy(dg_h, wd.at[:, pl.ds(0, FF)], lsem.at[4]),
-        pltpu.make_async_copy(du_h, wd.at[:, pl.ds(FF, FF)], lsem.at[5]),
-        pltpu.make_async_copy(dd_h.at[:, pl.ds(pl.multiple_of(t * Q, Q), Q)], dd, lsem.at[6]),
+    pairs = [
+        (lens_h, lens), (ids_h, ids_t), (rw_h, rw_t), (inv_h, inv), (resid_h, resid), (ga_h, gain_a),
+        (wq_h, wqkv.at[:, pl.ds(0, Q)]),
+        (wk_h, wqkv.at[:, pl.ds(Q, HEAD_DIM)]),
+        (wv_h, wqkv.at[:, pl.ds(Q + HEAD_DIM, HEAD_DIM)]),
+        (lam_h, lam), (hgain_h, hgain),
     ]
+    pairs += [(kv_h.at[pl.ds(4 * g, 4)], kv.at[pl.ds(4 * g, 4)]) for g in range(4)]
+    pairs += [
+        (wo_h, wo), (gf_h, gain), (mixw_h, mix_w), (ed_h, ed),
+        (eg_h, we.at[:, pl.ds(0, FF)]), (eu_h, we.at[:, pl.ds(FF, FF)]),
+        (dg_h, wd.at[:, pl.ds(0, FF)]), (du_h, wd.at[:, pl.ds(FF, FF)]),
+        (dd_h.at[:, pl.ds(pl.multiple_of(t * Q, Q), Q)], dd),
+    ]
+    loads = [pltpu.make_async_copy(a, b, lsem.at[i]) for i, (a, b) in enumerate(pairs)]
     for load in loads:
         load.start()
+    KV0 = 11
+    WO = KV0 + 4
 
     barrier = pltpu.get_barrier_semaphore()
     peers = (
@@ -133,6 +92,9 @@
     )
     for peer in peers:
         pl.semaphore_signal(barrier, inc=1, device_id=peer, device_id_type=MESH)
+
+    for load in loads[:4]:
+        load.wait()
 
     ids_f = ids_t[...].astype(F32)
     rw = rw_t[...]
@@ -168,6 +130,84 @@
     for i, field in enumerate(fields):
         info = jnp.where(lane == i, field, info)
 
+    lane1 = lax.broadcasted_iota(jnp.int32, (SEQ, HEAD_DIM), 1)
+    length = column(lens[...].astype(F32), 0)
+    lenb[...] = jnp.broadcast_to(length, (SEQ, HEAD_DIM))
+    angle = length * inv[...]
+    cosine = jnp.cos(angle)
+    low = lax.rem(lane1, QK_DIM) < QK_DIM // 2
+    sine = jnp.where(low, -jnp.sin(angle), jnp.sin(angle))
+
+    def turned(v):
+        ahead = pltpu.roll(v, HEAD_DIM - QK_DIM // 2, 1)
+        behind = pltpu.roll(v, QK_DIM // 2, 1)
+        return (v * cosine + jnp.where(low, ahead, behind) * sine).astype(BF16)
+
+    for load in loads[4:6]:
+        load.wait()
+    normed = rms_rows(resid[...].astype(F32), gain_a[...]).astype(BF16)
+    for load in loads[6:KV0]:
+        load.wait()
+    proj = dot(normed, wqkv[...])
+    key_new = turned(proj[:, Q : Q + HEAD_DIM])
+    val_new = proj[:, Q + HEAD_DIM :].astype(BF16)
+    rows_out[:, 0:HEAD_DIM] = key_new
+    rows_out[:, HEAD_DIM:] = val_new
+    fk[...] = key_new.astype(F32)
+    fv[...] = val_new.astype(F32)
+    first = lane1 < QK_DIM
+    turned_q = [turned(proj[:, j * HEAD_DIM : (j + 1) * HEAD_DIM]) for j in range(4)]
+    zero = jnp.zeros((SEQ, HEAD_DIM), BF16)
+    stack = jnp.concatenate(
+        [jnp.where(first, q, zero) for q in turned_q] + [jnp.where(first, zero, q) for q in turned_q],
+        axis=0,
+    )
+    prow = lax.broadcasted_iota(jnp.int32, (128, 128), 0)
+    pcol = lax.broadcasted_iota(jnp.int32, (128, 128), 1)
+    to_seq = lax.rem(prow, 8) * SEQ + lax.div(prow, 8) == pcol
+    to_head = lax.rem(prow, SEQ) * 8 + lax.div(prow, SEQ) == pcol
+    qs[...] = dot(jnp.where(to_seq, 1.0, 0.0).astype(BF16), stack).reshape(SEQ, 8, HEAD_DIM)
+
+    srow = lax.broadcasted_iota(jnp.int32, (8, 4), 0)
+    scol = lax.broadcasted_iota(jnp.int32, (8, 4), 1)
+    lam_col = jnp.sum(
+        jnp.where(srow - 4 == scol, jnp.broadcast_to(lam[...], (8, 4)), 0.0), axis=1, keepdims=True
+    )
+    sign = jnp.where(lax.broadcasted_iota(jnp.int32, (8, 1), 0) < 4, 1.0, -lam_col)
+    position = lax.broadcasted_iota(jnp.int32, (8, 512), 1).astype(F32)
+    scale = QK_DIM ** (-0.5)
+
+    def four_sequences(g, carry):
+        pltpu.make_async_copy(
+            kv_h.at[pl.ds(4 * g, 4)], kv.at[pl.ds(4 * g, 4)], lsem.at[KV0 + g]
+        ).wait()
+        for i in range(4):
+            b = 4 * g + i
+            qb = qs[b]
+            scores = scale * lax.dot_general(
+                qb.astype(BF16), kv[b, :, 0:HEAD_DIM], (((1,), (1,)), ((), ())),
+                preferred_element_type=F32,
+            )
+            latest = scale * jnp.sum(qb * fk[pl.ds(b, 1), :], axis=1, keepdims=True)
+            valid = position < lenb[pl.ds(b, 1), 0:1]
+            masked = jnp.where(valid, scores, -1e30)
+            top = jnp.maximum(jnp.max(masked, axis=1, keepdims=True), latest)
+            raised = jnp.where(valid, jnp.exp(masked - top), 0.0)
+            raised_new = jnp.exp(latest - top)
+            weight = sign / (jnp.sum(raised, axis=1, keepdims=True) + raised_new)
+            both = raised * weight
+            mapped = (both + pltpu.roll(both, 4, 0)).astype(BF16)
+            new = raised_new * weight
+            mapped_new = (new + pltpu.roll(jnp.broadcast_to(new, (8, HEAD_DIM)), 4, 0)).astype(BF16)
+            mixed[b] = dot(mapped, kv[b, :, HEAD_DIM:]) + mapped_new.astype(F32) * fv[pl.ds(b, 1), :]
+        return carry
+
+    lax.fori_loop(0, 4, four_sequences, 0)
+    normed_heads = rms_rows(mixed[...].reshape(128, HEAD_DIM), hgain[...]).astype(BF16)
+    by_head = dot(jnp.where(to_head, 1.0, 0.0).astype(BF16), normed_heads).astype(BF16)
+    for j in range(4):
+        heads[:, j * HEAD_DIM : (j + 1) * HEAD_DIM] = by_head[j * SEQ : (j + 1) * SEQ, :]
+
     pl.semaphore_wait(barrier, 14)
 
     heads_out = [
@@ -175,15 +215,9 @@
     ]
     for copy in heads_out:
         copy.start()
-    loads[0].wait()
-    ed_out = []
-    for k in (1, 2, 3):
-        cols = pl.ds(pl.multiple_of(up(t, k, NY) * Q, Q), Q)
-        copy = remote(ed.at[:, cols], edx.at[t], ed_s.at[k - 1], ed_r.at[k - 1], dev(dy=k))
-        copy.start()
-        ed_out.append(copy)
     own_cols = pl.ds(pl.multiple_of(t * Q, Q), Q)
-    loads[1].wait()
+    for load in loads[WO:WO + 4]:
+        load.wait()
 
     def wo_rows(src):
         return wo[pl.ds(pl.multiple_of(src * Q, Q), Q), :]
@@ -200,6 +234,12 @@
     ]
     for copy in cols_out:
         copy.start()
+    ed_out = []
+    for k in (1, 2, 3):
+        cols = pl.ds(pl.multiple_of(up(t, k, NY) * Q, Q), Q)
+        copy = remote(ed.at[:, cols], edx.at[t], ed_s.at[k - 1], ed_r.at[k - 1], dev(dy=k))
+        copy.start()
+        ed_out.append(copy)
     for k in (1, 3, 2):
         src = up(t, -k, NY)
         remote(sg.at[src], sg.at[src], c_s.at[k - 1], c_r.at[k - 1], dev()).wait_recv()
@@ -291,7 +331,7 @@
 
     lax.fori_loop(0, NX * NZ, sibling_arrival, 0)
 
-    for load in loads[2:]:
+    for load in loads[WO + 4:]:
         load.wait()
     e_f = e.astype(F32)
     brow = lax.broadcasted_iota(jnp.int32, (INFO, INFO), 0)
@@ -418,18 +458,39 @@
     lax.fori_loop(0, N_SENDS, sent, 0)
 
 
-def tail(*operands):
+def layer(*operands):
     vmem = pl.BlockSpec(memory_space=pltpu.VMEM)
-    hbm = pl.BlockSpec(memory_space=pl.ANY)
+    hbm = pl.BlockSpec(memory_space=pltpu.HBM)
     rows = NC * NZ * SEQ
     dma = lambda *n: pltpu.SemaphoreType.DMA(n)
     buf = lambda shape, kind=BF16: pltpu.VMEM(shape, kind)
     return pl.pallas_call(
-        tail_kernel,
-        out_shape=jax.ShapeDtypeStruct((SEQ, Q), F32),
-        in_specs=[vmem] * 6 + [hbm] * 7,
-        out_specs=vmem,
+        layer_kernel,
+        out_shape=(
+            jax.ShapeDtypeStruct((SEQ, Q), F32),
+            jax.ShapeDtypeStruct((SEQ, 2 * HEAD_DIM), BF16),
+        ),
+        in_specs=[hbm] * len(operands),
+        out_specs=(vmem, vmem),
         scratch_shapes=[
+            buf((SEQ, D)),
+            buf((1, SEQ), jnp.int32),
+            buf((SEQ, 512, 2 * HEAD_DIM)),
+            buf((1, D), F32),
+            buf((D, Q + 2 * HEAD_DIM)),
+            buf((1, 4), F32),
+            buf((1, HEAD_DIM), F32),
+            buf((1, D), F32),
+            buf((2, SEQ), jnp.int32),
+            buf((2, SEQ), F32),
+            buf((1, D), F32),
+            buf((1, HEAD_DIM), F32),
+            buf((SEQ, 8, HEAD_DIM), F32),
+            buf((SEQ, HEAD_DIM), F32),
+            buf((SEQ, HEAD_DIM), F32),
+            buf((SEQ, HEAD_DIM), F32),
+            buf((SEQ, 8, HEAD_DIM), F32),
+            buf((SEQ, Q)),
             buf((D, Q)),
             buf((D, 2 * FF)),
             buf((D, 2 * FF)),
@@ -455,15 +516,15 @@
             buf((NZ, SEQ, Q), F32),
             buf((NZ, SEQ, Q)),
             buf((NZ - 1, SEQ, Q)),
-            dma(7),
+            dma(24),
             dma(3), dma(3), dma(3), dma(3), dma(3), dma(3),
             dma(N_SENDS), dma(NX, NC, NZ),
             dma(3), dma(3), dma(4), dma(4), dma(3), dma(3), dma(7), dma(7),
         ],
         compiler_params=pltpu.CompilerParams(
-            collective_id=0, has_side_effects=True, vmem_limit_bytes=48 * 1024 * 1024
+            collective_id=0, has_side_effects=True, vmem_limit_bytes=60 * 1024 * 1024
         ),
-        name="tail",
+        name="layer",
     )(*operands)
 
 
@@ -472,36 +533,34 @@
     diff_lambda, head_gain, out_weight, norm_gain_ffn, route_ids, route_weights, expert_gate,
     expert_up, expert_down, dense_gate, dense_up, dense_down, dense_mix,
 ):
-    seq_count, width = residual_in.shape
-    groups = kv_cache.shape[1]
-    local_heads = diff_lambda.shape[0]
-    resid = residual_in.astype(F32)
-    normed = rms_rows(resid, norm_gain_attn).astype(BF16)
-    positions = lengths.astype(F32)
-    query = dot(normed, query_weight).reshape(seq_count, local_heads, 2, QK_DIM)
-    query = rotate(query, positions).astype(BF16)
-    keys = dot(normed, key_weight).reshape(seq_count, groups, 2, QK_DIM)
-    keys = rotate(keys, positions).astype(BF16).reshape(seq_count, groups, 2 * QK_DIM)
-    values = dot(normed, value_weight).reshape(seq_count, groups, HEAD_DIM).astype(BF16)
-    fresh = jnp.concatenate([keys, values], axis=-1)
-    mixed = attend(query, fresh, kv_cache, lengths, diff_lambda)
-    heads_out = rms_rows(mixed, head_gain).astype(BF16).reshape(seq_count, local_heads * HEAD_DIM)
-    final = tail(
-        heads_out,
+    width = residual_in.shape[1]
+    half = QK_DIM // 2
+    inverse = 10000.0 ** (-np.arange(half, dtype=np.float32) / np.float32(half))
+    inverse = np.tile(inverse.astype(np.float32), 4)[None, :]
+    final, fresh = layer(
         residual_in,
+        lengths.reshape(1, -1),
+        kv_cache.reshape(SEQ, 512, 2 * HEAD_DIM),
+        norm_gain_attn.reshape(1, width),
+        query_weight,
+        key_weight,
+        value_weight,
+        diff_lambda.reshape(1, -1),
+        head_gain.reshape(1, -1),
+        out_weight,
         norm_gain_ffn.reshape(1, width),
-        dense_mix.reshape(1, width),
         route_ids.T,
         route_weights.T,
-        out_weight,
         expert_gate.reshape(width, -1),
         expert_up.reshape(width, -1),
         expert_down.reshape(-1, width),
         dense_gate,
         dense_up,
         dense_down,
-    )
-    return (final.astype(BF16), fresh)
+        dense_mix.reshape(1, width),
+        jnp.asarray(inverse),
+    )
+    return (final.astype(BF16), fresh.reshape(SEQ, 1, 2 * HEAD_DIM))
 
 
 def solution(mesh):

time: 80.9 us -> 74.5 us (0.921)
  matrix products: 9.09 us -> 0 us
  Pallas kernels: 65.8 us -> 71 us
  other arithmetic: 3.33 us -> 1.37 us
    dot_general x8 -> x0, matrix products: 9.09 us -> none  [the longest x4 5.06 us: scores(): jnp.einsum(eq, grouped[:, :, :, lo], keys, preferred_element_type=F32)]
    pallas_call x1, Pallas kernels: 65.8 us -> 71 us  [layer(): pl.pallas_call(layer_kernel, out_shape=(jax.ShapeDtypeStruct((SEQ, Q), F3...]
    reduce_sum x2 -> x0, other arithmetic: 1.43 us -> none  [the longest x1 1.11 us: rms_rows(): mean_sq = jnp.mean(values * values, axis=-1, keepdims=True)]
where the time goes in v2:
time: 74.5 us; the launch traced here: 74.3 us
  Pallas kernels  71 us (95%)
  other arithmetic  1.37 us (2%)
  local copies, waits for them, and re-layouts  1.29 us (2%)
    pallas_call x1, Pallas kernels, layer(): pl.pallas_call(layer_kernel, out_shape=(jax.ShapeDtypeStruct((SEQ, Q), F3...  71 us

profile of v2, /device:TPU:1, one launch (start us, length us, event | category | flops | bytes accessed | tf_op | source)
XLA Modules:
  0.0 74.3 jit_solution(5569165301958701269)
XLA Ops:
  0.6 71.0 %layer.1 = (f32[16,512]{1,0:T(8,128)}, bf16[16,256]{1,0:T(8,128)(2,1)}) custom-call(bf16[16,2048]{1,0:T(8,128)(2,1)} %resid_h.1, s32[1,16]{1,0:T(1,128)} %bitcast.23, bf16[16,512,256]{2,1,0:T(8,128)(2,1)} %bitcast.13, f32[1,2048]{1,0:T(1,128)} %bitcast.17, bf16[2048,512]{1,0:T(8,128)(2,1)} %wq_h.1, bf16[2048,128]{1,0:T(8,128)(2,1)} %wk_h.1, ...), custom_call_target="tpu_custom_call" | custom-call | tf_op jit(solution)/shard_map/layer/pallas_call | solution.py:467
  71.6 1.4 %convert_element_type.3 = bf16[16,512]{1,0:T(8,128)(2,1)} convert(f32[16,512]{1,0:T(8,128)} %get-tuple-element.4) | non-fusion elementwise | flops 8192 | bytes 49152 | tf_op jit(solution)/shard_map/convert_element_type | solution.py:563
  73.0 1.3 %copy.24 = bf16[16,1,256]{2,0,1:T(8,128)(2,1)} copy(bf16[16,1,256]{2,0,1:T(8,128)(2,1)} %bitcast.20) | data formatting | bytes 16384

commit v3 on v2

--- a/solution.py
+++ b/solution.py
@@ -20,7 +20,9 @@
 WIDE = D + INFO
 FF = 128
 X_ORDER = (0, 1, 3, 2)
-N_SENDS = 63
+Z_ORDER = (0, -1, 1, -2, 2, -3, 3, 4)
+N_SENDS = 67
+NOT_SENT = tuple(15 + 32 + 4 * j + (2 if j < 2 else 0) for j in range(4))
 
 
 def rms_rows(values, gain):
@@ -32,8 +34,8 @@
     return jnp.dot(a, b, preferred_element_type=F32)
 
 
-def up(v, n, size):
-    return lax.rem(v + (n % size), size)
+def up(v, n, size, dynamic=False):
+    return lax.rem(v + (n if dynamic else n % size), size)
 
 
 def layer_kernel(
@@ -41,7 +43,7 @@
     eg_h, eu_h, ed_h, dg_h, du_h, dd_h, mixw_h, inv_h, out, rows_out,
     resid, lens, kv, gain_a, wqkv, lam, hgain, gain, ids_t, rw_t, mix_w, inv,
     qs, fk, fv, lenb, mixed, heads,
-    wo, we, wd, ed, dd, edx, hg, sg, xg, he, hd, st, wc, mc, hx, slots, eo,
+    wo, w4, spread, ed, dd, edx, hg, sg, xg, hd, st, wc, mc, hx, slots, eo,
     s0, r0, own, s1, r1, bsum, s2, r2,
     lsem, ed_s, ed_r, h_s, h_r, c_s, c_r, g_s, g_r, x_s, x_r, s0_s, s0_r, s1_s, s1_r, s2_s, s2_r,
 ):
@@ -73,8 +75,8 @@
     pairs += [(kv_h.at[pl.ds(4 * g, 4)], kv.at[pl.ds(4 * g, 4)]) for g in range(4)]
     pairs += [
         (wo_h, wo), (gf_h, gain), (mixw_h, mix_w), (ed_h, ed),
-        (eg_h, we.at[:, pl.ds(0, FF)]), (eu_h, we.at[:, pl.ds(FF, FF)]),
-        (dg_h, wd.at[:, pl.ds(0, FF)]), (du_h, wd.at[:, pl.ds(FF, FF)]),
+        (eg_h, w4.at[:, pl.ds(0, FF)]), (eu_h, w4.at[:, pl.ds(FF, FF)]),
+        (dg_h, w4.at[:, pl.ds(2 * FF, FF)]), (du_h, w4.at[:, pl.ds(3 * FF, FF)]),
         (dd_h.at[:, pl.ds(pl.multiple_of(t * Q, Q), Q)], dd),
     ]
     loads = [pltpu.make_async_copy(a, b, lsem.at[i]) for i, (a, b) in enumerate(pairs)]
@@ -174,35 +176,40 @@
         jnp.where(srow - 4 == scol, jnp.broadcast_to(lam[...], (8, 4)), 0.0), axis=1, keepdims=True
     )
     sign = jnp.where(lax.broadcasted_iota(jnp.int32, (8, 1), 0) < 4, 1.0, -lam_col)
-    position = lax.broadcasted_iota(jnp.int32, (8, 512), 1).astype(F32)
+    sign4 = jnp.concatenate([sign] * 4, axis=0)
+    position = lax.broadcasted_iota(jnp.int32, (32, 512), 1).astype(F32)
     scale = QK_DIM ** (-0.5)
-
-    def four_sequences(g, carry):
-        pltpu.make_async_copy(
-            kv_h.at[pl.ds(4 * g, 4)], kv.at[pl.ds(4 * g, 4)], lsem.at[KV0 + g]
-        ).wait()
-        for i in range(4):
-            b = 4 * g + i
-            qb = qs[b]
-            scores = scale * lax.dot_general(
-                qb.astype(BF16), kv[b, :, 0:HEAD_DIM], (((1,), (1,)), ((), ())),
-                preferred_element_type=F32,
-            )
-            latest = scale * jnp.sum(qb * fk[pl.ds(b, 1), :], axis=1, keepdims=True)
-            valid = position < lenb[pl.ds(b, 1), 0:1]
-            masked = jnp.where(valid, scores, -1e30)
-            top = jnp.maximum(jnp.max(masked, axis=1, keepdims=True), latest)
-            raised = jnp.where(valid, jnp.exp(masked - top), 0.0)
-            raised_new = jnp.exp(latest - top)
-            weight = sign / (jnp.sum(raised, axis=1, keepdims=True) + raised_new)
-            both = raised * weight
-            mapped = (both + pltpu.roll(both, 4, 0)).astype(BF16)
-            new = raised_new * weight
-            mapped_new = (new + pltpu.roll(jnp.broadcast_to(new, (8, HEAD_DIM)), 4, 0)).astype(BF16)
-            mixed[b] = dot(mapped, kv[b, :, HEAD_DIM:]) + mapped_new.astype(F32) * fv[pl.ds(b, 1), :]
-        return carry
-
-    lax.fori_loop(0, 4, four_sequences, 0)
+    contract_last = (((1,), (1,)), ((), ()))
+    for load in loads[KV0:WO]:
+        load.wait()
+    for g in range(4):
+        seqs = range(4 * g, 4 * g + 4)
+        q4 = [qs[b] for b in seqs]
+        scores = jnp.concatenate(
+            [
+                lax.dot_general(
+                    q.astype(BF16), kv[b, :, 0:HEAD_DIM], contract_last, preferred_element_type=F32
+                )
+                for q, b in zip(q4, seqs)
+            ],
+            axis=0,
+        )
+        latest = scale * jnp.concatenate(
+            [jnp.sum(q * fk[b : b + 1, :], axis=1, keepdims=True) for q, b in zip(q4, seqs)], axis=0
+        )
+        count = jnp.concatenate([jnp.broadcast_to(lenb[b : b + 1, 0:1], (8, 1)) for b in seqs], axis=0)
+        masked = jnp.where(position < count, scores * scale, -1e30)
+        top = jnp.maximum(jnp.max(masked, axis=1, keepdims=True), latest)
+        raised = jnp.exp(masked - top)
+        raised_new = jnp.exp(latest - top)
+        weight = sign4 / (jnp.sum(raised, axis=1, keepdims=True) + raised_new)
+        both = raised * weight
+        mapped = (both + pltpu.roll(both, 28, 0)).astype(BF16)
+        new = jnp.broadcast_to(raised_new * weight, (32, HEAD_DIM))
+        mapped_new = (new + pltpu.roll(new, 28, 0)).astype(BF16).astype(F32)
+        for i, b in enumerate(seqs):
+            at = slice(8 * i, 8 * i + 8)
+            mixed[b] = dot(mapped[at, :], kv[b, :, HEAD_DIM:]) + mapped_new[at, :] * fv[b : b + 1, :]
     normed_heads = rms_rows(mixed[...].reshape(128, HEAD_DIM), hgain[...]).astype(BF16)
     by_head = dot(jnp.where(to_head, 1.0, 0.0).astype(BF16), normed_heads).astype(BF16)
     for j in range(4):
@@ -251,144 +258,184 @@
     xg[x, c, z, :, 0:D] = ffn_in
     xg[x, c, z, :, D:WIDE] = info.astype(BF16)
 
-    counter = [0]
-
-    def send(px, pc, pz, **to):
-        i = counter[0]
-        counter[0] += 1
-        remote(xg.at[px, pc, pz], xg.at[px, pc, pz], g_s.at[i], g_r.at[px, pc, pz], dev(**to)).start()
-
-    def arrive(px, pc, pz):
-        ref = xg.at[px, pc, pz]
-        remote(ref, ref, g_s.at[0], g_r.at[px, pc, pz], dev()).wait_recv()
-
-    @pl.when(c == 0)
-    def _():
-        counter[0] = 0
-        for k in (1, 3, 2):
-            send(x, 0, z, dx=k)
-        send(x, 0, z, dz=1)
-        send(x, 0, z, dz=-1)
-        send(x, 0, z, flip=True)
-        for k in (1, 3, 2):
-            px = up(x, k, NX)
-            arrive(px, 0, z)
-            send(px, 0, z, dz=1)
-            send(px, 0, z, dz=-1)
-            send(px, 0, z, flip=True)
-        for step in (1, 2, 3):
-            for j, k in enumerate(X_ORDER):
-                px = up(x, k, NX)
-                for sign in (1, -1):
-                    pz = up(z, -sign * step, NZ)
-                    arrive(px, 0, pz)
-                    if step < 3 or (j < 2) == (sign == 1):
-                        send(px, 0, pz, dz=sign)
-                    send(px, 0, pz, flip=True)
-        for k in X_ORDER:
-            px = up(x, k, NX)
-            pz = up(z, 4, NZ)
-            arrive(px, 0, pz)
-            send(px, 0, pz, flip=True)
-        assert counter[0] == N_SENDS
-
-    @pl.when(c == 1)
-    def _():
-        counter[0] = 0
-        z_order = [0, -1, 1, -2, 2, -3, 3, 4]
-        for m, k in enumerate(z_order):
-            pz = up(z, k, NZ)
-            if m:
-                arrive(x, 1, pz)
-            if m == 0:
-                send(x, 1, pz, dz=1)
-                send(x, 1, pz, dz=-1)
-            elif k < 0:
-                send(x, 1, pz, dz=1)
-            elif k < 3:
-                send(x, 1, pz, dz=-1)
-            send(x, 1, pz, dx=1)
-            send(x, 1, pz, dx=-1)
-            send(x, 1, pz, flip=True)
-        for m, k in enumerate(z_order):
-            pz = up(z, k, NZ)
-            for sign in (1, -1):
-                px = up(x, -sign, NX)
-                arrive(px, 1, pz)
-                if (m % 2 == 0) == (sign == 1):
-                    send(px, 1, pz, dx=sign)
-                send(px, 1, pz, flip=True)
-        for k in z_order:
-            px = up(x, 2, NX)
-            pz = up(z, k, NZ)
-            arrive(px, 1, pz)
-            send(px, 1, pz, flip=True)
-        assert counter[0] == N_SENDS
-
-    def sibling_arrival(i, carry):
-        arrive(lax.div(i, NZ), 1 - c, lax.rem(i, NZ))
-        return carry
-
-    lax.fori_loop(0, NX * NZ, sibling_arrival, 0)
-
-    for load in loads[WO + 4:]:
+    slots[...] = jnp.zeros_like(slots)
+    for load in loads[WO + 4 :]:
         load.wait()
     e_f = e.astype(F32)
     brow = lax.broadcasted_iota(jnp.int32, (INFO, INFO), 0)
     spans = ((0, 1), (1, 2), (2, 3), (3, 4), (4, 7), (7, 10), (10, 13))
-    spread = jnp.concatenate(
-        [jnp.where((brow >= lo) & (brow < hi), 1.0, 0.0).astype(BF16) for lo, hi in spans], axis=1
-    )
-    rows = NC * NZ * SEQ
-    rr = lax.broadcasted_iota(jnp.int32, (rows, INFO), 0)
-    ll = lax.broadcasted_iota(jnp.int32, (rows, INFO), 1)
-    rel = (ll - 2 * lax.div(rr, SEQ)).astype(F32)
-
-    def expert_rows(i, carry):
-        block = xg[i].reshape(rows, WIDE)
-        both = dot(block[:, 0:D], we[...])
-        hidden = (jax.nn.silu(both[:, 0:FF]) * both[:, FF:]).astype(BF16)
-        b = dot(block[:, D:WIDE], spread)
+    for i, (lo, hi) in enumerate(spans):
+        spread[:, i * INFO : (i + 1) * INFO] = jnp.where((brow >= lo) & (brow < hi), 1.0, 0.0).astype(BF16)
+    grow = lax.div(lax.broadcasted_iota(jnp.int32, (128, INFO), 0), SEQ)
+    glane = lax.broadcasted_iota(jnp.int32, (128, INFO), 1)
+
+    def group(block, base):
+        both = dot(block[:, 0:D], w4[...])
+        hidden = (jax.nn.silu(both[:, 0:FF]) * both[:, FF : 2 * FF]).astype(BF16)
+        dense = (jax.nn.silu(both[:, 2 * FF : 3 * FF]) * both[:, 3 * FF :]).astype(BF16)
+        b = dot(block[:, D:WIDE], spread[...])
         part = [b[:, k * INFO : (k + 1) * INFO] for k in range(7)]
         m0 = part[0] == e_f
         m1 = part[1] == e_f
-        wc[i] = jnp.where(m0, part[4], 0.0) + jnp.where(m1, part[5], 0.0)
-        mc[i] = part[6]
+        weight = jnp.where(m0, part[4], 0.0) + jnp.where(m1, part[5], 0.0)
         slot = jnp.where(m0, part[2], jnp.where(m1, part[3], -4096.0))
-        base = (i * (2 * NC * NZ)).astype(F32)
-        chosen = jnp.where(slot == rel - base, 1.0, 0.0).astype(BF16)
-        st[i] = chosen
-        he[...] = hidden
-        got = lax.dot_general(
-            st[i], he[...], (((0,), (0,)), ((), ())), preferred_element_type=F32
+        chosen = jnp.where(slot == (glane - base).astype(F32), 1.0, 0.0).astype(BF16)
+        slots[...] += lax.dot_general(
+            chosen, hidden, (((0,), (0,)), ((), ())), preferred_element_type=F32
         )
-
-        @pl.when(i == 0)
-        def _():
-            slots[...] = got
-
-        @pl.when(i > 0)
-        def _():
-            slots[...] += got
-
-        return carry
-
-    lax.fori_loop(0, NX, expert_rows, 0)
+        return dense, chosen, weight, part[6]
+
+    def z_group(step):
+        ahead = up(z, lax.rem(step, 4), NZ, True)
+        behind = up(z, NZ - step, NZ, True)
+        block = jnp.concatenate(
+            [xg[:, 1, ahead].reshape(64, WIDE), xg[:, 1, behind].reshape(64, WIDE)], axis=0
+        )
+        column_of = jnp.where(grow < 4, ahead, behind)
+        base = 2 * NC * NZ * lax.rem(grow, 4) + 2 * NZ + 2 * column_of
+        for ref, value in zip((hd, st, wc, mc), group(block, base)):
+            ref[:, 1, ahead] = value[0:64].reshape(NX, SEQ, INFO)
+            ref[:, 1, behind] = value[64:].reshape(NX, SEQ, INFO)
+
+    def x_group(d):
+        px = up(x, d, NX, True)
+        base = 2 * NC * NZ * px + 2 * grow
+        for ref, value in zip((hd, st, wc, mc), group(xg[px, 0].reshape(128, WIDE), base)):
+            ref[px, 0] = value.reshape(NZ, SEQ, INFO)
+
+    def x_rank(i):
+        return i + jnp.where(i == 2, 1, 0) - jnp.where(i == 3, 1, 0)
+
+    def send(i, px, pc, pz, **to):
+        remote(xg.at[px, pc, pz], xg.at[px, pc, pz], g_s.at[i], g_r.at[px, pc, pz], dev(**to)).start()
+
+    def arrive(px, pc, pz):
+        ref = xg.at[px, pc, pz]
+        remote(ref, ref, g_s.at[0], g_r.at[px, pc, pz], dev()).wait_recv()
+
+    def z_rank(m):
+        far = lax.div(m + 1, 2)
+        return lax.rem(jnp.where(lax.rem(m, 2) == 1, NZ - far, far), NZ)
+
+    @pl.when(c == 1)
+    def _():
+        send(0, x, 1, z, dx=2)
+        send(1, x, 1, z, dx=1)
+        send(2, x, 1, z, dx=-1)
+        send(3, x, 1, z, dz=1)
+        send(4, x, 1, z, dz=-1)
+        send(5, x, 1, z, flip=True)
+        for m, k in enumerate((1, 3, 2)):
+            px = up(x, k, NX)
+            arrive(px, 1, z)
+            send(6 + 3 * m, px, 1, z, dz=1)
+            send(7 + 3 * m, px, 1, z, dz=-1)
+            send(8 + 3 * m, px, 1, z, flip=True)
+
+        def ring_step(step, carry):
+            back = up(z, NZ - step, NZ, True)
+            front = up(z, step, NZ, True)
+            first = 15 + 16 * (step - 1)
+
+            @pl.when(step < 4)
+            def _():
+                for j, k in enumerate(X_ORDER):
+                    px = up(x, k, NX)
+                    for way, (pz, sign) in enumerate(((back, 1), (front, -1))):
+                        at = first + 4 * j + 2 * way
+                        arrive(px, 1, pz)
+                        if (j < 2) == (sign == 1):
+                            send(at, px, 1, pz, dz=sign)
+                        else:
+
+                            @pl.when(step < 3)
+                            def _():
+                                send(at, px, 1, pz, dz=sign)
+
+                        send(at + 1, px, 1, pz, flip=True)
+
+            @pl.when(step == 4)
+            def _():
+                for j, k in enumerate(X_ORDER):
+                    px = up(x, k, NX)
+                    arrive(px, 1, front)
+                    send(first + j, px, 1, front, flip=True)
+
+            z_group(step)
+            return carry
+
+        lax.fori_loop(1, 5, ring_step, 0)
+
+        def other_core(i, carry):
+            px = up(x, x_rank(i), NX, True)
+            for pz in range(NZ):
+                arrive(px, 0, pz)
+            x_group(x_rank(i))
+            return carry
+
+        lax.fori_loop(0, NX, other_core, 0)
+        for i in range(15 + 16 * 3 + 4):
+            if i in NOT_SENT:
+                continue
+            remote(xg.at[0, 0, 0], xg.at[0, 0, 0], g_s.at[i], g_r.at[0, 0, 0], dev()).wait_send()
+
+    @pl.when(c == 0)
+    def _():
+        n = 0
+        for m, k in enumerate(Z_ORDER):
+            pz = up(z, k, NZ)
+            if m:
+                arrive(x, 0, pz)
+            if m == 0:
+                send(n, x, 0, pz, dz=1)
+                send(n + 1, x, 0, pz, dz=-1)
+                n += 2
+            elif k < 3:
+                send(n, x, 0, pz, dz=1 if k < 0 else -1)
+                n += 1
+            send(n, x, 0, pz, dx=1)
+            send(n + 1, x, 0, pz, dx=-1)
+            send(n + 2, x, 0, pz, flip=True)
+            n += 3
+        for m, k in enumerate(Z_ORDER):
+            pz = up(z, k, NZ)
+            for sign in (1, -1):
+                px = up(x, -sign, NX)
+                arrive(px, 0, pz)
+                if (m % 2 == 0) == (sign == 1):
+                    send(n, px, 0, pz, dx=sign)
+                    n += 1
+                send(n, px, 0, pz, flip=True)
+                n += 1
+
+        def last_steps(i, carry):
+            px = up(x, 2, NX)
+            for m in range(2):
+                pz = up(z, z_rank(2 * i + m), NZ, True)
+                arrive(px, 0, pz)
+                send(n + 2 * i + m, px, 0, pz, flip=True)
+            x_group(x_rank(i))
+            step = i + 1
+            for pz in (up(z, lax.rem(step, 4), NZ, True), up(z, NZ - step, NZ, True)):
+                for k in range(NX):
+                    arrive(k, 1, pz)
+            z_group(step)
+            return carry
+
+        lax.fori_loop(0, NX, last_steps, 0)
+
+        def sent(i, carry):
+            remote(xg.at[0, 0, 0], xg.at[0, 0, 0], g_s.at[i], g_r.at[0, 0, 0], dev()).wait_send()
+            return carry
+
+        lax.fori_loop(0, n + 8, sent, 0)
+
     hx[t] = slots[...].astype(BF16)
     hid_out = [
         remote(hx.at[t], hx.at[t], x_s.at[k - 1], x_r.at[k - 1], dev(dy=k)) for k in (1, 2, 3)
     ]
     for copy in hid_out:
         copy.start()
-
-    def dense_rows(i, carry):
-        block = xg[i].reshape(rows, WIDE)
-        both = dot(block[:, 0:D], wd[...])
-        hd[i] = (jax.nn.silu(both[:, 0:FF]) * both[:, FF:]).astype(BF16)
-        return carry
-
-    lax.fori_loop(0, NX, dense_rows, 0)
-
     edx[t] = ed[:, own_cols]
     for k in (1, 3, 2):
         src = up(t, -k, NY)
@@ -399,37 +446,49 @@
         result = result + dot(hx[k], edx[k]).astype(BF16).astype(F32)
     eo[...] = result.astype(BF16)
 
-    half = NZ * SEQ
+    rows = NZ * SEQ
 
     def part_of(px, pc):
-        at = pl.ds(pl.multiple_of(pc * half, half), half)
-        four = lambda a: jnp.concatenate([a] * 4, axis=1)
-        dense = dot(hd[px, at, :], dd[...])
-        routed = dot(st[px, at, :], eo[...])
-        return four(mc[px, at, :]) * dense + four(wc[px, at, :]) * routed
-
-    x_seq = (2, 1, 3, 0)
+        four = lambda ref: jnp.concatenate([ref[px, pc].reshape(rows, INFO)] * 4, axis=1)
+        dense = dot(hd[px, pc].reshape(rows, FF), dd[...])
+        routed = dot(st[px, pc].reshape(rows, INFO), eo[...])
+        return four(mc) * dense + four(wc) * routed
+
     pair_out = {}
-    for k in x_seq:
+    for k in (2, 1, 3, 0):
         px = up(x, k, NX)
         s0[k] = part_of(px, 1 - c).astype(BF16)
         pair_out[k] = remote(s0.at[k], r0.at[k], s0_s.at[k], s0_r.at[k], dev(flip=True))
         pair_out[k].start()
         own[k] = part_of(px, c)
-    x_out = {}
-    for k in x_seq:
+    left = slice(0, Q // 2)
+    right = slice(Q // 2, Q)
+    x_out = []
+
+    def x_send(i, value, dx):
+        s1[i] = value.astype(BF16)
+        copy = remote(s1.at[i], r1.at[i], s1_s.at[i], s1_r.at[i], dev(dx=dx))
+        copy.start()
+        x_out.append(copy)
+
+    def x_got(i):
+        remote(s1.at[i], r1.at[i], s1_s.at[i], s1_r.at[i], dev()).wait_recv()
+        return r1[i].astype(F32)
+
+    for k in (2, 1, 3, 0):
         pair_out[k].wait_recv()
-        joined = own[k] + r0[k].astype(F32)
-        if k:
-            s1[k - 1] = joined.astype(BF16)
-            x_out[k] = remote(s1.at[k - 1], r1.at[k - 1], s1_s.at[k - 1], s1_r.at[k - 1], dev(dx=k))
-            x_out[k].start()
-        else:
-            own[0] = joined
-    sums = own[0]
-    for k in (1, 3, 2):
-        x_out[k].wait_recv()
-        sums = sums + r1[k - 1].astype(F32)
+        own[k] = own[k] + r0[k].astype(F32)
+        if k == 2:
+            x_send(0, own[2, :, left], 1)
+            x_send(1, own[2, :, right], -1)
+        elif k == 1:
+            x_send(2, own[1, :, right], 1)
+        elif k == 3:
+            x_send(3, own[3, :, left], -1)
+    x_send(4, own[1, :, left] + x_got(0), 1)
+    x_send(5, own[3, :, right] + x_got(1), -1)
+    from_below = [own[0, :, left] + x_got(3), own[0, :, right] + x_got(2)]
+    sums = jnp.concatenate([from_below[0] + x_got(4), from_below[1] + x_got(5)], axis=1)
     bsum[...] = sums.reshape(NZ, SEQ, Q)
     s2[...] = sums.astype(BF16).reshape(NZ, SEQ, Q)
     z_out = []
@@ -447,21 +506,13 @@
 
     for copy in heads_out + ed_out + cols_out + hid_out + list(pair_out.values()):
         copy.wait_send()
-    for copy in list(x_out.values()) + z_out:
+    for copy in x_out + z_out:
         copy.wait_send()
-
-    def sent(i, carry):
-        ref = xg.at[0, 0, 0]
-        remote(ref, ref, g_s.at[i], g_r.at[0, 0, 0], dev()).wait_send()
-        return carry
-
-    lax.fori_loop(0, N_SENDS, sent, 0)
 
 
 def layer(*operands):
     vmem = pl.BlockSpec(memory_space=pltpu.VMEM)
     hbm = pl.BlockSpec(memory_space=pltpu.HBM)
-    rows = NC * NZ * SEQ
     dma = lambda *n: pltpu.SemaphoreType.DMA(n)
     buf = lambda shape, kind=BF16: pltpu.VMEM(shape, kind)
     return pl.pallas_call(
@@ -492,34 +543,33 @@
             buf((SEQ, 8, HEAD_DIM), F32),
             buf((SEQ, Q)),
             buf((D, Q)),
-            buf((D, 2 * FF)),
-            buf((D, 2 * FF)),
+            buf((D, 4 * FF)),
+            buf((INFO, 7 * INFO)),
             buf((FF, D)),
             buf((FF, Q)),
             buf((NY, FF, Q)),
             buf((NY, SEQ, Q)),
             buf((NY, SEQ, Q)),
             buf((NX, NC, NZ, SEQ, WIDE)),
-            buf((rows, FF)),
-            buf((NX, rows, FF)),
-            buf((NX, rows, INFO)),
-            buf((NX, rows, INFO), F32),
-            buf((NX, rows, INFO), F32),
+            buf((NX, NC, NZ, SEQ, FF)),
+            buf((NX, NC, NZ, SEQ, INFO)),
+            buf((NX, NC, NZ, SEQ, INFO), F32),
+            buf((NX, NC, NZ, SEQ, INFO), F32),
             buf((NY, 128, FF)),
             buf((128, FF), F32),
             buf((128, Q)),
             buf((NX, NZ * SEQ, Q)),
             buf((NX, NZ * SEQ, Q)),
             buf((NX, NZ * SEQ, Q), F32),
-            buf((NX - 1, NZ * SEQ, Q)),
-            buf((NX - 1, NZ * SEQ, Q)),
+            buf((6, NZ * SEQ, Q // 2)),
+            buf((6, NZ * SEQ, Q // 2)),
             buf((NZ, SEQ, Q), F32),
             buf((NZ, SEQ, Q)),
             buf((NZ - 1, SEQ, Q)),
             dma(24),
             dma(3), dma(3), dma(3), dma(3), dma(3), dma(3),
             dma(N_SENDS), dma(NX, NC, NZ),
-            dma(3), dma(3), dma(4), dma(4), dma(3), dma(3), dma(7), dma(7),
+            dma(3), dma(3), dma(4), dma(4), dma(6), dma(6), dma(7), dma(7),
         ],
         compiler_params=pltpu.CompilerParams(
             collective_id=0, has_side_effects=True, vmem_limit_bytes=60 * 1024 * 1024

time: 74.5 us -> 70.5 us (0.946); the launches traced: 74.3 us -> 69.5 us
  Pallas kernels: 71 us -> 66.2 us
    pallas_call x1, Pallas kernels: 71 us -> 66.2 us  [layer(): pl.pallas_call(layer_kernel, out_shape=(jax.ShapeDtypeStruct((SEQ, Q), F3...]
where the time goes in v3:
time: 70.5 us; the launch traced here: 69.5 us
  Pallas kernels  66.2 us (94%)
  other arithmetic  1.37 us (2%)
  local copies, waits for them, and re-layouts  1.29 us (2%)
    pallas_call x1, Pallas kernels, layer(): pl.pallas_call(layer_kernel, out_shape=(jax.ShapeDtypeStruct((SEQ, Q), F3...  66.2 us

profile of v3, /device:TPU:1, one launch (start us, length us, event | category | flops | bytes accessed | tf_op | source)
XLA Modules:
  0.0 69.5 jit_solution(4985131429673125533)
XLA Ops:
  0.6 66.2 %layer.1 = (f32[16,512]{1,0:T(8,128)}, bf16[16,256]{1,0:T(8,128)(2,1)}) custom-call(bf16[16,2048]{1,0:T(8,128)(2,1)} %resid_h.1, s32[1,16]{1,0:T(1,128)} %bitcast.23, bf16[16,512,256]{2,1,0:T(8,128)(2,1)} %bitcast.13, f32[1,2048]{1,0:T(1,128)} %bitcast.17, bf16[2048,512]{1,0:T(8,128)(2,1)} %wq_h.1, bf16[2048,128]{1,0:T(8,128)(2,1)} %wk_h.1, ...), custom_call_target="tpu_custom_call" | custom-call | tf_op jit(solution)/shard_map/layer/pallas_call | solution.py:518
  66.8 1.4 %convert_element_type.3 = bf16[16,512]{1,0:T(8,128)(2,1)} convert(f32[16,512]{1,0:T(8,128)} %get-tuple-element.4) | non-fusion elementwise | flops 8192 | bytes 49152 | tf_op jit(solution)/shard_map/convert_element_type | solution.py:613
  68.2 1.3 %copy.24 = bf16[16,1,256]{2,0,1:T(8,128)(2,1)} copy(bf16[16,1,256]{2,0,1:T(8,128)(2,1)} %bitcast.20) | data formatting | bytes 16384

commit v4 on v3

v4 whole, which is shorter than its diff:
```python
import jax
import jax.numpy as jnp
import numpy as np
from jax import lax
from jax.experimental import pallas as pl
from jax.experimental.pallas import tpu as pltpu
from jax.sharding import PartitionSpec as P

QK_DIM = 64
HEAD_DIM = 128
EPS = 1e-06
MESH = pl.DeviceIdType.MESH
F32 = jnp.float32
BF16 = jnp.bfloat16
NX, NZ, NY, NC = 4, 8, 4, 2
SEQ = 16
D = 2048
Q = 512
FF = 128
Z_ORDER = (0, -1, 1, -2, 2, -3, 3, 4)
FAR_FIRST = (4, 3, 5, 2, 6, 1, 7)
N_SENDS = 63


def rms_rows(values, gain):
    mean_sq = jnp.mean(values * values, axis=-1, keepdims=True)
    return values * lax.rsqrt(mean_sq + EPS) * gain


def dot(a, b):
    return jnp.dot(a, b, preferred_element_type=F32)


def up(v, n, size, dynamic=False):
    return lax.rem(v + (n if dynamic else n % size), size)


def layer_kernel(
    resid_h, lens_h, kv_h, ga_h, wq_h, wk_h, wv_h, lam_h, hgain_h, wo_h, gf_h, ids_h, rw_h,
    eg_h, eu_h, ed_h, dg_h, du_h, dd_h, mixw_h, inv_h, out, rows_out,
    resid, lens, kv, gain_a, wqkv, lam, hgain, gain, ids_t, rw_t, mix_w, inv,
    qs, fk, fv, lenb, mixed, heads,
    wo, we, wd, ddq, ed, edx, hg, sg, perm, m1s, m1r, m2s, my, hx, eo, n1r, n2s, n2r,
    xd, hd, s0, r0, own, s1, r1, bsum, s2, r2, ys, yr,
    lsem, ed_s, ed_r, h_s, h_r, c_s, c_r, x_s, x_r, y_s, y_r, g_s, g_r, m1_s, m1_q, m2_s, m2_q,
    my_s, my_r, n1_s, n1_q, n2_s, n2_q, s0_s, s0_r, s1_s, s1_r, s2_s, s2_r,
):
    e = lax.axis_index("ep")
    t = lax.axis_index("tp")
    z = lax.div(e, 8)
    x = lax.rem(lax.div(e, 2), 4)
    c = lax.rem(e, 2)

    def dev(dz=0, dx=0, flip=0, dy=0):
        cc = 1 - c if flip else c
        return {
            "ep": (up(z, dz, NZ) * NX + up(x, dx, NX)) * NC + cc,
            "tp": up(t, dy, NY),
        }

    def remote(src, dst, ssem, rsem, to):
        return pltpu.make_async_remote_copy(
            src_ref=src, dst_ref=dst, send_sem=ssem, recv_sem=rsem, device_id=to, device_id_type=MESH
        )

    pairs = [
        (lens_h, lens), (ids_h, ids_t), (rw_h, rw_t), (inv_h, inv), (resid_h, resid), (ga_h, gain_a),
        (wq_h, wqkv.at[:, pl.ds(0, Q)]),
        (wk_h, wqkv.at[:, pl.ds(Q, HEAD_DIM)]),
        (wv_h, wqkv.at[:, pl.ds(Q + HEAD_DIM, HEAD_DIM)]),
        (lam_h, lam), (hgain_h, hgain),
    ]
    pairs += [(kv_h.at[pl.ds(4 * g, 4)], kv.at[pl.ds(4 * g, 4)]) for g in range(4)]
    pairs += [
        (wo_h, wo), (gf_h, gain), (mixw_h, mix_w), (ed_h, ed),
        (eg_h, we.at[:, pl.ds(0, FF)]), (eu_h, we.at[:, pl.ds(FF, FF)]),
        (dg_h, wd.at[:, pl.ds(0, FF)]), (du_h, wd.at[:, pl.ds(FF, FF)]),
    ]
    pairs += [(dd_h.at[:, pl.ds(q * Q, Q)], ddq.at[q]) for q in range(NY)]
    loads = [pltpu.make_async_copy(a, b, lsem.at[i]) for i, (a, b) in enumerate(pairs)]
    for load in loads:
        load.start()
    KV0 = 11
    WO = KV0 + 4

    barrier = pltpu.get_barrier_semaphore()
    peers = (
        [dev(dy=k) for k in (1, 2, 3)]
        + [dev(dx=k) for k in (1, 2, 3)]
        + [dev(dz=k) for k in range(1, 8)]
        + [dev(dx=k, flip=1) for k in (0, 1, 2, 3)]
    )
    for peer in peers:
        pl.semaphore_signal(barrier, inc=1, device_id=peer, device_id_type=MESH)

    for load in loads[:4]:
        load.wait()

    ids = ids_t[...]
    place = ((ids >> 1) & 3) * (NC * NZ * 2) + (ids & 1) * (NZ * 2) + (ids >> 3) * 2
    row16 = lax.broadcasted_iota(jnp.int32, (SEQ, SEQ), 0)
    col16 = lax.broadcasted_iota(jnp.int32, (SEQ, SEQ), 1)
    eye = row16 == col16

    def column(rows, k):
        spread = jnp.broadcast_to(rows[k : k + 1, :], (SEQ, SEQ))
        return jnp.sum(jnp.where(eye, spread, 0.0), axis=1, keepdims=True)

    lane_f = lax.broadcasted_iota(jnp.int32, (SEQ, 128), 1).astype(F32)
    rw = rw_t[...]
    w_cols = [column(rw, k) for k in (0, 1)]
    place_cols = [column(place.astype(F32), k) for k in (0, 1)]
    member = [jnp.where(lane_f == col, 1.0, 0.0) for col in place_cols]
    before = jnp.where(row16 > col16, 1.0, 0.0).astype(BF16)
    earlier = dot(before, (member[0] + member[1]).astype(BF16))
    chosen = []
    for k in (0, 1):
        slot = jnp.sum(member[k] * earlier, axis=1, keepdims=True)
        chosen.append(jnp.where(lane_f == place_cols[k] + slot, 1.0, 0.0).astype(BF16))
    prow = lax.broadcasted_iota(jnp.int32, (128, 128), 0)
    pcol = lax.broadcasted_iota(jnp.int32, (128, 128), 1)
    swapped = ((prow >> 1) & 7) * 16 + (prow >> 4) * 2 + (prow & 1)
    perm[...] = jnp.where(pcol == swapped, 1.0, 0.0).astype(BF16)

    lane1 = lax.broadcasted_iota(jnp.int32, (SEQ, HEAD_DIM), 1)
    length = column(lens[...].astype(F32), 0)
    lenb[...] = jnp.broadcast_to(length, (SEQ, HEAD_DIM))
    angle = length * inv[...]
    cosine = jnp.cos(angle)
    low = lax.rem(lane1, QK_DIM) < QK_DIM // 2
    sine = jnp.where(low, -jnp.sin(angle), jnp.sin(angle))

    def turned(v):
        ahead = pltpu.roll(v, HEAD_DIM - QK_DIM // 2, 1)
        behind = pltpu.roll(v, QK_DIM // 2, 1)
        return (v * cosine + jnp.where(low, ahead, behind) * sine).astype(BF16)

    for load in loads[4:6]:
        load.wait()
    normed = rms_rows(resid[...].astype(F32), gain_a[...]).astype(BF16)
    for load in loads[6:KV0]:
        load.wait()
    proj = dot(normed, wqkv[...])
    key_new = turned(proj[:, Q : Q + HEAD_DIM])
    val_new = proj[:, Q + HEAD_DIM :].astype(BF16)
    rows_out[:, 0:HEAD_DIM] = key_new
    rows_out[:, HEAD_DIM:] = val_new
    fk[...] = key_new.astype(F32)
    fv[...] = val_new.astype(F32)
    first = lane1 < QK_DIM
    turned_q = [turned(proj[:, j * HEAD_DIM : (j + 1) * HEAD_DIM]) for j in range(4)]
    zero = jnp.zeros((SEQ, HEAD_DIM), BF16)
    stack = jnp.concatenate(
        [jnp.where(first, q, zero) for q in turned_q] + [jnp.where(first, zero, q) for q in turned_q],
        axis=0,
    )
    to_seq = lax.rem(prow, 8) * SEQ + lax.div(prow, 8) == pcol
    to_head = lax.rem(prow, SEQ) * 8 + lax.div(prow, SEQ) == pcol
    qs[...] = dot(jnp.where(to_seq, 1.0, 0.0).astype(BF16), stack).reshape(SEQ, 8, HEAD_DIM)

    srow = lax.broadcasted_iota(jnp.int32, (8, 4), 0)
    scol = lax.broadcasted_iota(jnp.int32, (8, 4), 1)
    lam_col = jnp.sum(
        jnp.where(srow - 4 == scol, jnp.broadcast_to(lam[...], (8, 4)), 0.0), axis=1, keepdims=True
    )
    sign = jnp.where(lax.broadcasted_iota(jnp.int32, (8, 1), 0) < 4, 1.0, -lam_col)
    sign4 = jnp.concatenate([sign] * 4, axis=0)
    position = lax.broadcasted_iota(jnp.int32, (32, 512), 1).astype(F32)
    scale = QK_DIM ** (-0.5)
    contract_last = (((1,), (1,)), ((), ()))
    for load in loads[KV0:WO]:
        load.wait()
    for g in range(4):
        seqs = range(4 * g, 4 * g + 4)
        q4 = [qs[b] for b in seqs]
        scores = jnp.concatenate(
            [
                lax.dot_general(
                    q.astype(BF16), kv[b, :, 0:HEAD_DIM], contract_last, preferred_element_type=F32
                )
                for q, b in zip(q4, seqs)
            ],
            axis=0,
        )
        latest = scale * jnp.concatenate(
            [jnp.sum(q * fk[b : b + 1, :], axis=1, keepdims=True) for q, b in zip(q4, seqs)], axis=0
        )
        count = jnp.concatenate([jnp.broadcast_to(lenb[b : b + 1, 0:1], (8, 1)) for b in seqs], axis=0)
        masked = jnp.where(position < count, scores * scale, -1e30)
        top = jnp.maximum(jnp.max(masked, axis=1, keepdims=True), latest)
        raised = jnp.exp(masked - top)
        raised_new = jnp.exp(latest - top)
        weight = sign4 / (jnp.sum(raised, axis=1, keepdims=True) + raised_new)
        both = raised * weight
        mapped = (both + pltpu.roll(both, 28, 0)).astype(BF16)
        new = jnp.broadcast_to(raised_new * weight, (32, HEAD_DIM))
        mapped_new = (new + pltpu.roll(new, 28, 0)).astype(BF16).astype(F32)
        for i, b in enumerate(seqs):
            at = slice(8 * i, 8 * i + 8)
            mixed[b] = dot(mapped[at, :], kv[b, :, HEAD_DIM:]) + mapped_new[at, :] * fv[b : b + 1, :]
    normed_heads = rms_rows(mixed[...].reshape(128, HEAD_DIM), hgain[...]).astype(BF16)
    by_head = dot(jnp.where(to_head, 1.0, 0.0).astype(BF16), normed_heads).astype(BF16)
    for j in range(4):
        heads[:, j * HEAD_DIM : (j + 1) * HEAD_DIM] = by_head[j * SEQ : (j + 1) * SEQ, :]

    pl.semaphore_wait(barrier, 17)

    heads_out = [
        remote(heads, hg.at[t], h_s.at[k - 1], h_r.at[k - 1], dev(dy=k)) for k in (1, 2, 3)
    ]
    for copy in heads_out:
        copy.start()
    own_cols = pl.ds(pl.multiple_of(t * Q, Q), Q)
    for load in loads[WO:WO + 4]:
        load.wait()

    def wo_rows(src):
        return wo[pl.ds(pl.multiple_of(src * Q, Q), Q), :]

    total = resid[:, own_cols].astype(F32) + dot(heads[...], wo_rows(t))
    for k in (1, 3, 2):
        src = up(t, -k, NY)
        remote(heads, hg.at[src], h_s.at[k - 1], h_r.at[k - 1], dev()).wait_recv()
        total = total + dot(hg[src], wo_rows(src))
    stream_cols = total.astype(BF16)
    sg[t] = stream_cols
    done = heads_out
    started = []

    def begin(src, dst, ssem, rsem, **to):
        copy = remote(src, dst, ssem, rsem, dev(**to))
        copy.start()
        started.append(copy)

    def landed(ref, rsem):
        remote(ref, ref, rsem, rsem, dev()).wait_recv()

    for k in (2, 1, 3):
        begin(sg.at[t], sg.at[t], c_s.at[k - 1], c_r.at[k - 1], dy=k)

    xc = x * NC + c
    outgoing = lax.dot_general(
        (chosen[0] + chosen[1]), stream_cols, (((0,), (0,)), ((), ())), preferred_element_type=F32
    )
    m1s[...] = outgoing.astype(BF16).reshape(NX * NC, SEQ, Q)
    plane = [(dx, flip) for dx in (2, 1, 3) for flip in (0, 1)] + [(0, 1)]

    def other(dx, flip):
        return up(x, dx, NX) * NC + (1 - c if flip else c)

    for i, (dx, flip) in enumerate(plane):
        begin(m1s.at[other(dx, flip)], m1r.at[xc], m1_s.at[i], m1_q.at[i], dx=dx, flip=flip)
    m1r[xc] = m1s[xc]
    for k in (2, 1, 3):
        cols = pl.ds(pl.multiple_of(up(t, k, NY) * Q, Q), Q)
        begin(ed.at[:, cols], edx.at[t], ed_s.at[k - 1], ed_r.at[k - 1], dy=k)

    for k in (1, 3, 2):
        src = up(t, -k, NY)
        landed(sg.at[src], c_r.at[k - 1])
    stream = jnp.concatenate([sg[k] for k in range(NY)], axis=1).astype(F32)
    ffn_in = rms_rows(stream, gain[...]).astype(BF16)
    mine = 4 * t + (row16 & 3) == col16
    block = jnp.zeros((SEQ, Q), F32)
    for q in range(NY):
        pick = jnp.where(mine & ((row16 >> 2) == q), 1.0, 0.0).astype(BF16)
        block = block + dot(pick, ffn_in[:, q * Q : (q + 1) * Q])
    xd[x, c, z] = block.astype(BF16)
    sends = [0]

    def give(px, pz, **to):
        i = sends[0]
        sends[0] += 1
        begin(xd.at[px, c, pz], xd.at[px, c, pz], g_s.at[i], g_r.at[px, c, pz], **to)

    def arrive(px, pc, pz):
        landed(xd.at[px, pc, pz], g_r.at[px, pc, pz])

    for k in FAR_FIRST:
        give(x, z, dz=k)
    give(x, z, dx=1)
    give(x, z, dx=-1)
    give(x, z, flip=1)
    mix = jax.nn.sigmoid(jnp.sum(ffn_in.astype(F32) * mix_w[...], axis=-1, keepdims=True))
    mix_row = jnp.sum(jnp.where(eye, jnp.broadcast_to(mix, (SEQ, SEQ)), 0.0), axis=0, keepdims=True)
    mix_mine = jnp.sum(jnp.where(mine, jnp.broadcast_to(mix_row, (SEQ, SEQ)), 0.0), axis=1, keepdims=True)

    def regroup(ref):
        return dot(perm[...], ref[...].reshape(128, Q)).astype(BF16).reshape(8, SEQ, Q)

    for i, (dx, flip) in enumerate(plane):
        landed(m1r.at[other(-dx, flip)], m1_q.at[i])
    m2s[...] = regroup(m1r)
    for k in FAR_FIRST:
        begin(m2s.at[up(z, k, NZ)], my.at[t, z], m2_s.at[k - 1], m2_q.at[k - 1], dz=k)
    my[t, z] = m2s[z]

    for k in Z_ORDER[1:]:
        pz = up(z, k, NZ)
        arrive(x, c, pz)
        give(x, pz, dx=1)
        give(x, pz, dx=-1)
        give(x, pz, flip=1)

    count = [0]

    def pass_on(pt, pz, dy):
        i = count[0]
        count[0] += 1
        begin(my.at[pt, pz], my.at[pt, pz], my_s.at[i], my_r.at[pt, pz], dy=dy)

    for k in Z_ORDER:
        pz = up(z, k, NZ)
        if k:
            landed(my.at[t, pz], m2_q.at[(-k) % NZ - 1])
        pass_on(t, pz, 1)
        pass_on(t, pz, -1)

    for m, k in enumerate(Z_ORDER):
        pz = up(z, k, NZ)
        for way in (1, -1):
            px = up(x, -way, NX)
            arrive(px, c, pz)
            if (m % 2 == 0) == (way == 1):
                give(px, pz, dx=way)
            give(px, pz, flip=1)
    for m, k in enumerate(Z_ORDER):
        pz = up(z, k, NZ)
        for way in (1, -1):
            pt = up(t, -way, NY)
            landed(my.at[pt, pz], my_r.at[pt, pz])
            if (m % 2 == 0) == (way == 1):
                pass_on(pt, pz, way)
    for k in Z_ORDER:
        pz = up(z, k, NZ)
        px = up(x, 2, NX)
        arrive(px, c, pz)
        give(px, pz, flip=1)

    for load in loads[WO + 4 :]:
        load.wait()
    drow = lax.broadcasted_iota(jnp.int32, (256, 1), 0)
    quarter = (drow >> 2) & 3
    low_rows = (lax.broadcasted_iota(jnp.int32, (128, 1), 0) & 7) < 4

    def by_quarter(value):
        which = quarter[0 : value.shape[0]]
        return jnp.concatenate([jnp.where(which == q, value, jnp.zeros_like(value)) for q in range(NY)], axis=1)

    def dense_rows(px):
        both = dot(by_quarter(xd[px].reshape(256, Q)), wd[...]).reshape(16, 2, 8, 2 * FF)
        half = (both[:, 0] + both[:, 1]).reshape(128, 2 * FF)
        full = half + jnp.where(low_rows, pltpu.roll(half, 124, 0), pltpu.roll(half, 4, 0))
        hidden = (jax.nn.silu(full[:, 0:FF]) * full[:, FF:]).reshape(16, 8, FF)
        hd[px] = jnp.concatenate([hidden, hidden], axis=1).astype(BF16).reshape(NC, NZ, SEQ, FF)

    def part_of(px, pc):
        return dot(by_quarter(hd[px, pc].reshape(128, FF)), ddq[...].reshape(NY * FF, Q))

    for k in (2, 1, 3, 0):
        px = up(x, k, NX)
        for pz in range(NZ):
            arrive(px, 1 - c, pz)
        dense_rows(px)
        s0[k] = part_of(px, 1 - c).astype(BF16)
        begin(s0.at[k], r0.at[k], s0_s.at[k], s0_r.at[k], flip=1)
        own[k] = part_of(px, c)

    for k in Z_ORDER:
        pz = up(z, k, NZ)
        pt = up(t, 2, NY)
        landed(my.at[pt, pz], my_r.at[pt, pz])
    rows_in = jnp.concatenate([my[k].reshape(128, Q) for k in range(NY)], axis=1).astype(F32)
    both = dot(rms_rows(rows_in, gain[...]).astype(BF16), we[...])
    hx[t] = (jax.nn.silu(both[:, 0:FF]) * both[:, FF:]).astype(BF16)
    for k in (2, 1, 3):
        begin(hx.at[t], hx.at[t], x_s.at[k - 1], x_r.at[k - 1], dy=k)

    left = slice(0, Q // 2)
    right = slice(Q // 2, Q)

    def x_send(i, value, dx):
        s1[i] = value.astype(BF16)
        begin(s1.at[i], r1.at[i], s1_s.at[i], s1_r.at[i], dx=dx)

    def x_got(i):
        landed(r1.at[i], s1_r.at[i])
        return r1[i].astype(F32)

    for k in (2, 1, 3, 0):
        landed(r0.at[k], s0_r.at[k])
        own[k] = own[k] + r0[k].astype(F32)
        if k == 2:
            x_send(0, own[2, :, left], 1)
            x_send(1, own[2, :, right], -1)
        elif k == 1:
            x_send(2, own[1, :, right], 1)
        elif k == 3:
            x_send(3, own[3, :, left], -1)
    x_send(4, own[1, :, left] + x_got(0), 1)
    x_send(5, own[3, :, right] + x_got(1), -1)

    own_q = pl.ds(pl.multiple_of(t * Q, Q), Q)
    edx[t] = ed[:, own_q]
    for k in (1, 3, 2):
        src = up(t, -k, NY)
        landed(edx.at[src], ed_r.at[k - 1])
        landed(hx.at[src], x_r.at[k - 1])
    result = jnp.zeros((128, Q), F32)
    for k in range(NY):
        result = result + dot(hx[k], edx[k]).astype(BF16).astype(F32)
    eo[...] = result.astype(BF16).reshape(NZ, SEQ, Q)
    for k in FAR_FIRST:
        begin(eo.at[up(z, k, NZ)], n1r.at[z], n1_s.at[k - 1], n1_q.at[k - 1], dz=k)
    n1r[z] = eo[z]

    from_sides = [own[0, :, left] + x_got(3), own[0, :, right] + x_got(2)]
    sums = jnp.concatenate([from_sides[0] + x_got(4), from_sides[1] + x_got(5)], axis=1)
    bsum[...] = sums.reshape(NZ, SEQ, Q)
    s2[...] = sums.astype(BF16).reshape(NZ, SEQ, Q)
    for k in FAR_FIRST:
        begin(s2.at[up(z, k, NZ)], r2.at[k - 1], s2_s.at[k - 1], s2_r.at[k - 1], dz=k)

    for k in reversed(FAR_FIRST):
        landed(n1r.at[up(z, -k, NZ)], n1_q.at[k - 1])
    n2s[...] = regroup(n1r)
    for i, (dx, flip) in enumerate(plane):
        begin(n2s.at[other(dx, flip)], n2r.at[xc], n2_s.at[i], n2_q.at[i], dx=dx, flip=flip)
    n2r[xc] = n2s[xc]

    for k in reversed(FAR_FIRST):
        landed(r2.at[k - 1], s2_r.at[k - 1])
    dense = bsum[z]
    for k in range(NZ - 1):
        dense = dense + r2[k].astype(F32)
    dense = dense * mix_mine
    for q in range(NY):
        four = dense[4 * q : 4 * q + 4, :]
        ys[q] = jnp.concatenate([four, four], axis=0)
    yr[t] = ys[t]
    for k in (2, 1, 3):
        begin(ys.at[up(t, k, NY)], yr.at[t], y_s.at[k - 1], y_r.at[k - 1], dy=k)

    for i, (dx, flip) in enumerate(plane):
        landed(n2r.at[other(-dx, flip)], n2_q.at[i])
    back = n2r[...].reshape(128, Q)
    final = stream_cols.astype(F32)
    moe = w_cols[0] * dot(chosen[0], back) + w_cols[1] * dot(chosen[1], back)
    for k in (1, 3, 2):
        src = up(t, -k, NY)
        landed(yr.at[src], y_r.at[k - 1])
    dense_cols = jnp.concatenate([yr[k, 0:4, :] for k in range(NY)], axis=0)
    out[...] = final + moe + dense_cols

    for copy in done + started:
        copy.wait_send()


def layer(*operands):
    vmem = pl.BlockSpec(memory_space=pltpu.VMEM)
    hbm = pl.BlockSpec(memory_space=pltpu.HBM)
    dma = lambda *n: pltpu.SemaphoreType.DMA(n)
    buf = lambda shape, kind=BF16: pltpu.VMEM(shape, kind)
    return pl.pallas_call(
        layer_kernel,
        out_shape=(
            jax.ShapeDtypeStruct((SEQ, Q), F32),
            jax.ShapeDtypeStruct((SEQ, 2 * HEAD_DIM), BF16),
        ),
        in_specs=[hbm] * len(operands),
        out_specs=(vmem, vmem),
        scratch_shapes=[
            buf((SEQ, D)),
            buf((1, SEQ), jnp.int32),
            buf((SEQ, 512, 2 * HEAD_DIM)),
            buf((1, D), F32),
            buf((D, Q + 2 * HEAD_DIM)),
            buf((1, 4), F32),
            buf((1, HEAD_DIM), F32),
            buf((1, D), F32),
            buf((2, SEQ), jnp.int32),
            buf((2, SEQ), F32),
            buf((1, D), F32),
            buf((1, HEAD_DIM), F32),
            buf((SEQ, 8, HEAD_DIM), F32),
            buf((SEQ, HEAD_DIM), F32),
            buf((SEQ, HEAD_DIM), F32),
            buf((SEQ, HEAD_DIM), F32),
            buf((SEQ, 8, HEAD_DIM), F32),
            buf((SEQ, Q)),
            buf((D, Q)),
            buf((D, 2 * FF)),
            buf((D, 2 * FF)),
            buf((NY, FF, Q)),
            buf((FF, D)),
            buf((NY, FF, Q)),
            buf((NY, SEQ, Q)),
            buf((NY, SEQ, Q)),
            buf((128, 128)),
            buf((8, SEQ, Q)),
            buf((8, SEQ, Q)),
            buf((8, SEQ, Q)),
            buf((NY, NZ, SEQ, Q)),
            buf((NY, 128, FF)),
            buf((8, SEQ, Q)),
            buf((8, SEQ, Q)),
            buf((8, SEQ, Q)),
            buf((8, SEQ, Q)),
            buf((NX, NC, NZ, SEQ, Q)),
            buf((NX, NC, NZ, SEQ, FF)),
            buf((NX, NZ * SEQ, Q)),
            buf((NX, NZ * SEQ, Q)),
            buf((NX, NZ * SEQ, Q), F32),
            buf((6, NZ * SEQ, Q // 2)),
            buf((6, NZ * SEQ, Q // 2)),
            buf((NZ, SEQ, Q), F32),
            buf((NZ, SEQ, Q)),
            buf((NZ - 1, SEQ, Q)),
            buf((NY, 8, Q), F32),
            buf((NY, 8, Q), F32),
            dma(27),
            dma(3), dma(3), dma(3), dma(3), dma(3), dma(3), dma(3), dma(3), dma(3), dma(3),
            dma(N_SENDS), dma(NX, NC, NZ),
            dma(7), dma(7), dma(7), dma(7),
            dma(24), dma(NY, NZ),
            dma(7), dma(7), dma(7), dma(7),
            dma(4), dma(4), dma(6), dma(6), dma(7), dma(7),
        ],
        compiler_params=pltpu.CompilerParams(
            collective_id=0, has_side_effects=True, vmem_limit_bytes=60 * 1024 * 1024
        ),
        name="layer",
    )(*operands)


def on_device(
    residual_in, lengths, kv_cache, norm_gain_attn, query_weight, key_weight, value_weight,
    diff_lambda, head_gain, out_weight, norm_gain_ffn, route_ids, route_weights, expert_gate,
    expert_up, expert_down, dense_gate, dense_up, dense_down, dense_mix,
):
    width = residual_in.shape[1]
    half = QK_DIM // 2
    inverse = 10000.0 ** (-np.arange(half, dtype=np.float32) / np.float32(half))
    inverse = np.tile(inverse.astype(np.float32), 4)[None, :]
    final, fresh = layer(
        residual_in,
        lengths.reshape(1, -1),
        kv_cache.reshape(SEQ, 512, 2 * HEAD_DIM),
        norm_gain_attn.reshape(1, width),
        query_weight,
        key_weight,
        value_weight,
        diff_lambda.reshape(1, -1),
        head_gain.reshape(1, -1),
        out_weight,
        norm_gain_ffn.reshape(1, width),
        route_ids.T,
        route_weights.T,
        expert_gate.reshape(width, -1),
        expert_up.reshape(width, -1),
        expert_down.reshape(-1, width),
        dense_gate,
        dense_up,
        dense_down,
        dense_mix.reshape(1, width),
        jnp.asarray(inverse),
    )
    return (final.astype(BF16), fresh.reshape(SEQ, 1, 2 * HEAD_DIM))


def solution(mesh):
    placed = (
        P("ep", None),
        P("ep"),
        P("ep", "tp", None, None),
        P(),
        P(None, "tp"),
        P(None, "tp"),
        P(None, "tp"),
        P("tp"),
        P(),
        P(None, "tp"),
        P(),
        P("ep", None),
        P("ep", None),
        P("ep", None, "tp"),
        P("ep", None, "tp"),
        P("ep", "tp", None),
        P(None, "ep"),
        P(None, "ep"),
        P("ep", None),
        P(),
    )
    return jax.shard_map(
        on_device,
        mesh=mesh,
        in_specs=placed,
        out_specs=(P("ep", "tp"), P("ep", "tp", None)),
        check_vma=False,
    )
```

time: 70.5 us -> 62.9 us (0.89); the launches traced: 69.5 us -> 62.7 us
  Pallas kernels: 66.2 us -> 59.4 us
    pallas_call x1, Pallas kernels: 66.2 us -> 59.4 us  [layer(): pl.pallas_call(layer_kernel, out_shape=(jax.ShapeDtypeStruct((SEQ, Q), F3...]
where the time goes in v4:
time: 62.9 us; the launch traced here: 62.7 us
  Pallas kernels  59.4 us (94%)
  other arithmetic  1.37 us (2%)
  local copies, waits for them, and re-layouts  1.29 us (2%)
  between operations  0.65 us (1%)
    pallas_call x1, Pallas kernels, layer(): pl.pallas_call(layer_kernel, out_shape=(jax.ShapeDtypeStruct((SEQ, Q), F3...  59.4 us
    convert_element_type x1, other arithmetic, on_device(): return (final.astype(BF16), fresh.reshape(SEQ, 1, 2 * HEAD_DIM))  1.37 us
    unnamed x1, local copies, waits for them, and re-layouts  1.29 us

profile of v4, /device:TPU:1, one launch (start us, length us, event | category | flops | bytes accessed | tf_op | source)
XLA Modules:
  0.0 62.7 jit_solution(677313107220125309)
XLA Ops:
  0.6 59.4 %layer.1 = (f32[16,512]{1,0:T(8,128)}, bf16[16,256]{1,0:T(8,128)(2,1)}) custom-call(bf16[16,2048]{1,0:T(8,128)(2,1)} %resid_h.1, s32[1,16]{1,0:T(1,128)} %bitcast.23, bf16[16,512,256]{2,1,0:T(8,128)(2,1)} %bitcast.13, f32[1,2048]{1,0:T(1,128)} %bitcast.17, bf16[2048,512]{1,0:T(8,128)(2,1)} %wq_h.1, bf16[2048,128]{1,0:T(8,128)(2,1)} %wk_h.1, ...), custom_call_target="tpu_custom_call" | custom-call | tf_op jit(solution)/shard_map/layer/pallas_call | solution.py:464
  60.0 1.4 %convert_element_type.3 = bf16[16,512]{1,0:T(8,128)(2,1)} convert(f32[16,512]{1,0:T(8,128)} %get-tuple-element.4) | non-fusion elementwise | flops 8192 | bytes 49152 | tf_op jit(solution)/shard_map/convert_element_type | solution.py:568
  61.4 1.3 %copy.24 = bf16[16,1,256]{2,0,1:T(8,128)(2,1)} copy(bf16[16,1,256]{2,0,1:T(8,128)(2,1)} %bitcast.20) | data formatting | bytes 16384

commit v5 on v4

--- a/solution.py
+++ b/solution.py
@@ -41,7 +41,7 @@
     resid, lens, kv, gain_a, wqkv, lam, hgain, gain, ids_t, rw_t, mix_w, inv,
     qs, fk, fv, lenb, mixed, heads,
     wo, we, wd, ddq, ed, edx, hg, sg, perm, m1s, m1r, m2s, my, hx, eo, n1r, n2s, n2r,
-    xd, hd, s0, r0, own, s1, r1, bsum, s2, r2, ys, yr,
+    xd, s0, r0, own, s1, r1, bsum, s2, r2, ys, yr,
     lsem, ed_s, ed_r, h_s, h_r, c_s, c_r, x_s, x_r, y_s, y_r, g_s, g_r, m1_s, m1_q, m2_s, m2_q,
     my_s, my_r, n1_s, n1_q, n2_s, n2_q, s0_s, s0_r, s1_s, s1_r, s2_s, s2_r,
 ):
@@ -63,25 +63,42 @@
             src_ref=src, dst_ref=dst, send_sem=ssem, recv_sem=rsem, device_id=to, device_id_type=MESH
         )
 
-    pairs = [
-        (lens_h, lens), (ids_h, ids_t), (rw_h, rw_t), (inv_h, inv), (resid_h, resid), (ga_h, gain_a),
-        (wq_h, wqkv.at[:, pl.ds(0, Q)]),
-        (wk_h, wqkv.at[:, pl.ds(Q, HEAD_DIM)]),
-        (wv_h, wqkv.at[:, pl.ds(Q + HEAD_DIM, HEAD_DIM)]),
-        (lam_h, lam), (hgain_h, hgain),
-    ]
-    pairs += [(kv_h.at[pl.ds(4 * g, 4)], kv.at[pl.ds(4 * g, 4)]) for g in range(4)]
-    pairs += [
-        (wo_h, wo), (gf_h, gain), (mixw_h, mix_w), (ed_h, ed),
-        (eg_h, we.at[:, pl.ds(0, FF)]), (eu_h, we.at[:, pl.ds(FF, FF)]),
-        (dg_h, wd.at[:, pl.ds(0, FF)]), (du_h, wd.at[:, pl.ds(FF, FF)]),
-    ]
-    pairs += [(dd_h.at[:, pl.ds(q * Q, Q)], ddq.at[q]) for q in range(NY)]
-    loads = [pltpu.make_async_copy(a, b, lsem.at[i]) for i, (a, b) in enumerate(pairs)]
-    for load in loads:
+    pairs = {
+        "wq": (wq_h, wqkv.at[:, pl.ds(0, Q)]),
+        "wk": (wk_h, wqkv.at[:, pl.ds(Q, HEAD_DIM)]),
+        "wv": (wv_h, wqkv.at[:, pl.ds(Q + HEAD_DIM, HEAD_DIM)]),
+        "resid": (resid_h, resid),
+        "gain_a": (ga_h, gain_a),
+        "lens": (lens_h, lens),
+        "inv": (inv_h, inv),
+        "ids": (ids_h, ids_t),
+        "rw": (rw_h, rw_t),
+        "lam": (lam_h, lam),
+        "hgain": (hgain_h, hgain),
+    }
+    for g in range(4):
+        pairs[f"kv{g}"] = (kv_h.at[pl.ds(4 * g, 4)], kv.at[pl.ds(4 * g, 4)])
+    pairs |= {
+        "wo": (wo_h, wo),
+        "gain": (gf_h, gain),
+        "mix": (mixw_h, mix_w),
+        "ed": (ed_h, ed),
+        "dg": (dg_h, wd.at[:, pl.ds(0, FF)]),
+        "du": (du_h, wd.at[:, pl.ds(FF, FF)]),
+        "eg": (eg_h, we.at[:, pl.ds(0, FF)]),
+        "eu": (eu_h, we.at[:, pl.ds(FF, FF)]),
+    }
+    for q in range(NY):
+        pairs[f"dd{q}"] = (dd_h.at[:, pl.ds(q * Q, Q)], ddq.at[q])
+    loads = {
+        name: pltpu.make_async_copy(a, b, lsem.at[i]) for i, (name, (a, b)) in enumerate(pairs.items())
+    }
+    for load in loads.values():
         load.start()
-    KV0 = 11
-    WO = KV0 + 4
+
+    def loaded(*names):
+        for name in names:
+            loads[name].wait()
 
     barrier = pltpu.get_barrier_semaphore()
     peers = (
@@ -93,8 +110,7 @@
     for peer in peers:
         pl.semaphore_signal(barrier, inc=1, device_id=peer, device_id_type=MESH)
 
-    for load in loads[:4]:
-        load.wait()
+    loaded("lens", "inv", "ids", "rw")
 
     ids = ids_t[...]
     place = ((ids >> 1) & 3) * (NC * NZ * 2) + (ids & 1) * (NZ * 2) + (ids >> 3) * 2
@@ -135,11 +151,9 @@
         behind = pltpu.roll(v, QK_DIM // 2, 1)
         return (v * cosine + jnp.where(low, ahead, behind) * sine).astype(BF16)
 
-    for load in loads[4:6]:
-        load.wait()
+    loaded("resid", "gain_a")
     normed = rms_rows(resid[...].astype(F32), gain_a[...]).astype(BF16)
-    for load in loads[6:KV0]:
-        load.wait()
+    loaded("wq", "wk", "wv", "lam", "hgain")
     proj = dot(normed, wqkv[...])
     key_new = turned(proj[:, Q : Q + HEAD_DIM])
     val_new = proj[:, Q + HEAD_DIM :].astype(BF16)
@@ -168,8 +182,7 @@
     position = lax.broadcasted_iota(jnp.int32, (32, 512), 1).astype(F32)
     scale = QK_DIM ** (-0.5)
     contract_last = (((1,), (1,)), ((), ()))
-    for load in loads[KV0:WO]:
-        load.wait()
+    loaded("kv0", "kv1", "kv2", "kv3")
     for g in range(4):
         seqs = range(4 * g, 4 * g + 4)
         q4 = [qs[b] for b in seqs]
@@ -211,8 +224,7 @@
     for copy in heads_out:
         copy.start()
     own_cols = pl.ds(pl.multiple_of(t * Q, Q), Q)
-    for load in loads[WO:WO + 4]:
-        load.wait()
+    loaded("wo", "gain", "mix", "ed")
 
     def wo_rows(src):
         return wo[pl.ds(pl.multiple_of(src * Q, Q), Q), :]
@@ -302,6 +314,29 @@
         give(x, pz, dx=-1)
         give(x, pz, flip=1)
 
+    loaded("dg", "du", "eg", "eu", *[f"dd{q}" for q in range(NY)])
+    quarter = (lax.broadcasted_iota(jnp.int32, (256, 1), 0) >> 2) & 3
+    low_rows = (lax.broadcasted_iota(jnp.int32, (128, 1), 0) & 7) < 4
+
+    def by_quarter(value):
+        return jnp.concatenate(
+            [jnp.where(quarter == q, value, jnp.zeros_like(value)) for q in range(NY)], axis=1
+        )
+
+    def dense_rows(k):
+        px = up(x, k, NX)
+        for pz in range(NZ):
+            arrive(px, 1 - c, pz)
+        both = dot(by_quarter(xd[px].reshape(256, Q)), wd[...]).reshape(16, 2, 8, 2 * FF)
+        half = (both[:, 0] + both[:, 1]).reshape(128, 2 * FF)
+        full = half + jnp.where(low_rows, pltpu.roll(half, 124, 0), pltpu.roll(half, 4, 0))
+        hidden = (jax.nn.silu(full[:, 0:FF]) * full[:, FF:]).reshape(16, 8, FF)
+        rows16 = jnp.concatenate([hidden, hidden], axis=1).astype(BF16).reshape(256, FF)
+        part = dot(by_quarter(rows16), ddq[...].reshape(NY * FF, Q))
+        s0[k] = jnp.where(c == 0, part[128:], part[0:128]).astype(BF16)
+        begin(s0.at[k], r0.at[k], s0_s.at[k], s0_r.at[k], flip=1)
+        own[k] = jnp.where(c == 0, part[0:128], part[128:])
+
     count = [0]
 
     def pass_on(pt, pz, dy):
@@ -324,6 +359,7 @@
             if (m % 2 == 0) == (way == 1):
                 give(px, pz, dx=way)
             give(px, pz, flip=1)
+    dense_rows(0)
     for m, k in enumerate(Z_ORDER):
         pz = up(z, k, NZ)
         for way in (1, -1):
@@ -331,40 +367,36 @@
             landed(my.at[pt, pz], my_r.at[pt, pz])
             if (m % 2 == 0) == (way == 1):
                 pass_on(pt, pz, way)
+    dense_rows(1)
     for k in Z_ORDER:
         pz = up(z, k, NZ)
         px = up(x, 2, NX)
         arrive(px, c, pz)
         give(px, pz, flip=1)
-
-    for load in loads[WO + 4 :]:
-        load.wait()
-    drow = lax.broadcasted_iota(jnp.int32, (256, 1), 0)
-    quarter = (drow >> 2) & 3
-    low_rows = (lax.broadcasted_iota(jnp.int32, (128, 1), 0) & 7) < 4
-
-    def by_quarter(value):
-        which = quarter[0 : value.shape[0]]
-        return jnp.concatenate([jnp.where(which == q, value, jnp.zeros_like(value)) for q in range(NY)], axis=1)
-
-    def dense_rows(px):
-        both = dot(by_quarter(xd[px].reshape(256, Q)), wd[...]).reshape(16, 2, 8, 2 * FF)
-        half = (both[:, 0] + both[:, 1]).reshape(128, 2 * FF)
-        full = half + jnp.where(low_rows, pltpu.roll(half, 124, 0), pltpu.roll(half, 4, 0))
-        hidden = (jax.nn.silu(full[:, 0:FF]) * full[:, FF:]).reshape(16, 8, FF)
-        hd[px] = jnp.concatenate([hidden, hidden], axis=1).astype(BF16).reshape(NC, NZ, SEQ, FF)
-
-    def part_of(px, pc):
-        return dot(by_quarter(hd[px, pc].reshape(128, FF)), ddq[...].reshape(NY * FF, Q))
-
-    for k in (2, 1, 3, 0):
-        px = up(x, k, NX)
-        for pz in range(NZ):
-            arrive(px, 1 - c, pz)
-        dense_rows(px)
-        s0[k] = part_of(px, 1 - c).astype(BF16)
-        begin(s0.at[k], r0.at[k], s0_s.at[k], s0_r.at[k], flip=1)
-        own[k] = part_of(px, c)
+    dense_rows(3)
+
+    left = slice(0, Q // 2)
+    right = slice(Q // 2, Q)
+
+    def x_send(i, value, dx):
+        s1[i] = value.astype(BF16)
+        begin(s1.at[i], r1.at[i], s1_s.at[i], s1_r.at[i], dx=dx)
+
+    def x_got(i):
+        landed(r1.at[i], s1_r.at[i])
+        return r1[i].astype(F32)
+
+    def joined(k):
+        landed(r0.at[k], s0_r.at[k])
+        own[k] = own[k] + r0[k].astype(F32)
+
+    joined(1)
+    x_send(2, own[1, :, right], 1)
+    dense_rows(2)
+    joined(3)
+    x_send(3, own[3, :, left], -1)
+    joined(0)
+
 
     for k in Z_ORDER:
         pz = up(z, k, NZ)
@@ -376,27 +408,9 @@
     for k in (2, 1, 3):
         begin(hx.at[t], hx.at[t], x_s.at[k - 1], x_r.at[k - 1], dy=k)
 
-    left = slice(0, Q // 2)
-    right = slice(Q // 2, Q)
-
-    def x_send(i, value, dx):
-        s1[i] = value.astype(BF16)
-        begin(s1.at[i], r1.at[i], s1_s.at[i], s1_r.at[i], dx=dx)
-
-    def x_got(i):
-        landed(r1.at[i], s1_r.at[i])
-        return r1[i].astype(F32)
-
-    for k in (2, 1, 3, 0):
-        landed(r0.at[k], s0_r.at[k])
-        own[k] = own[k] + r0[k].astype(F32)
-        if k == 2:
-            x_send(0, own[2, :, left], 1)
-            x_send(1, own[2, :, right], -1)
-        elif k == 1:
-            x_send(2, own[1, :, right], 1)
-        elif k == 3:
-            x_send(3, own[3, :, left], -1)
+    joined(2)
+    x_send(0, own[2, :, left], 1)
+    x_send(1, own[2, :, right], -1)
     x_send(4, own[1, :, left] + x_got(0), 1)
     x_send(5, own[3, :, right] + x_got(1), -1)
 
@@ -464,8 +478,8 @@
     return pl.pallas_call(
         layer_kernel,
         out_shape=(
-            jax.ShapeDtypeStruct((SEQ, Q), F32),
-            jax.ShapeDtypeStruct((SEQ, 2 * HEAD_DIM), BF16),
+            pltpu.VMEM((SEQ, Q), F32),
+            pltpu.VMEM((SEQ, 2 * HEAD_DIM), BF16),
         ),
         in_specs=[hbm] * len(operands),
         out_specs=(vmem, vmem),
@@ -507,7 +521,6 @@
             buf((8, SEQ, Q)),
             buf((8, SEQ, Q)),
             buf((NX, NC, NZ, SEQ, Q)),
-            buf((NX, NC, NZ, SEQ, FF)),
             buf((NX, NZ * SEQ, Q)),
             buf((NX, NZ * SEQ, Q)),
             buf((NX, NZ * SEQ, Q), F32),

time: 62.9 us -> 56.6 us (0.90)
  Pallas kernels: 59.4 us -> 54.2 us
  other arithmetic: 1.37 us -> 0.61 us
  local copies, waits for them, and re-layouts: 1.29 us -> 0.6 us
    pallas_call x1, Pallas kernels: 59.4 us -> 54.2 us  [layer(): pl.pallas_call(layer_kernel, out_shape=(pltpu.VMEM((SEQ, Q), F32), pltpu....]
    convert_element_type x1, other arithmetic: 1.37 us -> 0.61 us  [on_device(): return (final.astype(BF16), fresh.reshape(SEQ, 1, 2 * HEAD_DIM))]
    unnamed x1, local copies, waits for them, and re-layouts: 1.29 us -> 0.6 us
where the time goes in v5:
time: 56.6 us; the launch traced here: 56 us
  Pallas kernels  54.2 us (96%)
  between operations  0.65 us (1%)
  other arithmetic  0.61 us (1%)
  local copies, waits for them, and re-layouts  0.6 us (1%)
    pallas_call x1, Pallas kernels, layer(): pl.pallas_call(layer_kernel, out_shape=(pltpu.VMEM((SEQ, Q), F32), pltpu....  54.2 us

profile of v5, /device:TPU:1, one launch (start us, length us, event | category | flops | bytes accessed | tf_op | source)
XLA Modules:
  0.0 56.0 jit_solution(9177295718953217212)
XLA Ops:
  0.6 54.2 %layer.1 = (f32[16,512]{1,0:T(8,128)S(1)}, bf16[16,256]{1,0:T(8,128)(2,1)S(1)}) custom-call(bf16[16,2048]{1,0:T(8,128)(2,1)} %resid_h.1, s32[1,16]{1,0:T(1,128)} %bitcast.23, bf16[16,512,256]{2,1,0:T(8,128)(2,1)} %bitcast.14, f32[1,2048]{1,0:T(1,128)} %bitcast.18, bf16[2048,512]{1,0:T(8,128)(2,1)} %wq_h.1, bf16[2048,128]{1,0:T(8,128)(2,1)} %wk_h.1, ...), custom_call_target="tpu_custom_call" | custom-call | tf_op jit(solution)/shard_map/layer/pallas_call | solution.py:478
  54.8 0.6 %convert_element_type.3 = bf16[16,512]{1,0:T(8,128)(2,1)} convert(f32[16,512]{1,0:T(8,128)S(1)} %get-tuple-element.4) | non-fusion elementwise | flops 8192 | bytes 49152 | tf_op jit(solution)/shard_map/convert_element_type | solution.py:581
  55.4 0.6 %copy.24 = bf16[16,1,256]{2,0,1:T(8,128)(2,1)} copy(bf16[16,1,256]{2,0,1:T(8,128)(2,1)S(1)} %bitcast.13) | data formatting | bytes 16384

commit v6 on v5

--- a/solution.py
+++ b/solution.py
@@ -19,7 +19,7 @@
 FF = 128
 Z_ORDER = (0, -1, 1, -2, 2, -3, 3, 4)
 FAR_FIRST = (4, 3, 5, 2, 6, 1, 7)
-N_SENDS = 63
+N_SENDS = 56
 
 
 def rms_rows(values, gain):
@@ -41,8 +41,8 @@
     resid, lens, kv, gain_a, wqkv, lam, hgain, gain, ids_t, rw_t, mix_w, inv,
     qs, fk, fv, lenb, mixed, heads,
     wo, we, wd, ddq, ed, edx, hg, sg, perm, m1s, m1r, m2s, my, hx, eo, n1r, n2s, n2r,
-    xd, s0, r0, own, s1, r1, bsum, s2, r2, ys, yr,
-    lsem, ed_s, ed_r, h_s, h_r, c_s, c_r, x_s, x_r, y_s, y_r, g_s, g_r, m1_s, m1_q, m2_s, m2_q,
+    xd, cut, join, piece, raw, s0, r0, own, s1, r1, bsum, s2, r2, ys, yr,
+    lsem, ed_s, ed_r, h_s, h_r, c_s, c_r, x_s, x_r, y_s, y_r, g_s, g_r, p_s, p_r, m1_s, m1_q, m2_s, m2_q,
     my_s, my_r, n1_s, n1_q, n2_s, n2_q, s0_s, s0_r, s1_s, s1_r, s2_s, s2_r,
 ):
     e = lax.axis_index("ep")
@@ -64,15 +64,15 @@
         )
 
     pairs = {
-        "wq": (wq_h, wqkv.at[:, pl.ds(0, Q)]),
-        "wk": (wk_h, wqkv.at[:, pl.ds(Q, HEAD_DIM)]),
-        "wv": (wv_h, wqkv.at[:, pl.ds(Q + HEAD_DIM, HEAD_DIM)]),
-        "resid": (resid_h, resid),
-        "gain_a": (ga_h, gain_a),
         "lens": (lens_h, lens),
         "inv": (inv_h, inv),
         "ids": (ids_h, ids_t),
         "rw": (rw_h, rw_t),
+        "resid": (resid_h, resid),
+        "gain_a": (ga_h, gain_a),
+        "wq": (wq_h, wqkv.at[:, pl.ds(0, Q)]),
+        "wk": (wk_h, wqkv.at[:, pl.ds(Q, HEAD_DIM)]),
+        "wv": (wv_h, wqkv.at[:, pl.ds(Q + HEAD_DIM, HEAD_DIM)]),
         "lam": (lam_h, lam),
         "hgain": (hgain_h, hgain),
     }
@@ -106,6 +106,7 @@
         + [dev(dx=k) for k in (1, 2, 3)]
         + [dev(dz=k) for k in range(1, 8)]
         + [dev(dx=k, flip=1) for k in (0, 1, 2, 3)]
+        + [dev(dz=k, dy=j) for k in range(1, 8) for j in (1, 2, 3)]
     )
     for peer in peers:
         pl.semaphore_signal(barrier, inc=1, device_id=peer, device_id_type=MESH)
@@ -137,6 +138,16 @@
     pcol = lax.broadcasted_iota(jnp.int32, (128, 128), 1)
     swapped = ((prow >> 1) & 7) * 16 + (prow >> 4) * 2 + (prow & 1)
     perm[...] = jnp.where(pcol == swapped, 1.0, 0.0).astype(BF16)
+    orow = lax.broadcasted_iota(jnp.int32, (64, SEQ), 0)
+    ocol = lax.broadcasted_iota(jnp.int32, (64, SEQ), 1)
+    token_of = (orow >> 4) * 4 + (orow & 3) == ocol
+    for j in range(4):
+        cut[j] = jnp.where(token_of & (((orow >> 2) & 3) == j), 1.0, 0.0).astype(BF16)
+    jrow = lax.broadcasted_iota(jnp.int32, (256, 256), 0)
+    jcol = lax.broadcasted_iota(jnp.int32, (256, 256), 1)
+    source = ((jrow >> 4) & 3) * 64 + ((jrow >> 2) & 3) * 16 + (jrow >> 6) * 4 + (jrow & 3)
+    join[...] = jnp.where(jcol == source, 1.0, 0.0).astype(BF16)
+    low8 = lax.broadcasted_iota(jnp.int32, (8, 128), 0) < 4
 
     lane1 = lax.broadcasted_iota(jnp.int32, (SEQ, HEAD_DIM), 1)
     length = column(lens[...].astype(F32), 0)
@@ -216,7 +227,7 @@
     for j in range(4):
         heads[:, j * HEAD_DIM : (j + 1) * HEAD_DIM] = by_head[j * SEQ : (j + 1) * SEQ, :]
 
-    pl.semaphore_wait(barrier, 17)
+    pl.semaphore_wait(barrier, 38)
 
     heads_out = [
         remote(heads, hg.at[t], h_s.at[k - 1], h_r.at[k - 1], dev(dy=k)) for k in (1, 2, 3)
@@ -247,8 +258,17 @@
     def landed(ref, rsem):
         remote(ref, ref, rsem, rsem, dev()).wait_recv()
 
-    for k in (2, 1, 3):
-        begin(sg.at[t], sg.at[t], c_s.at[k - 1], c_r.at[k - 1], dy=k)
+    cols128 = [stream_cols[:, j * 128 : (j + 1) * 128] for j in range(4)]
+    cutting = sum(dot(cut[j], cols128[j]) for j in range(4))
+    piece[...] = cutting.astype(BF16).reshape(NY, SEQ, 128)
+    sent = 0
+    for dz in FAR_FIRST + (0,):
+        for dy in (2, 1, 3, 0):
+            if dz or dy:
+                src = piece.at[up(t, dy, NY)]
+                begin(src, raw.at[z, t], p_s.at[sent], p_r.at[z, t], dz=dz, dy=dy)
+                sent += 1
+    raw[z, t] = piece[t]
 
     xc = x * NC + c
     outgoing = lax.dot_general(
@@ -264,20 +284,15 @@
         begin(m1s.at[other(dx, flip)], m1r.at[xc], m1_s.at[i], m1_q.at[i], dx=dx, flip=flip)
     m1r[xc] = m1s[xc]
     for k in (2, 1, 3):
+        begin(sg.at[t], sg.at[t], c_s.at[k - 1], c_r.at[k - 1], dy=k)
+    for k in (2, 1, 3):
         cols = pl.ds(pl.multiple_of(up(t, k, NY) * Q, Q), Q)
         begin(ed.at[:, cols], edx.at[t], ed_s.at[k - 1], ed_r.at[k - 1], dy=k)
 
-    for k in (1, 3, 2):
-        src = up(t, -k, NY)
-        landed(sg.at[src], c_r.at[k - 1])
-    stream = jnp.concatenate([sg[k] for k in range(NY)], axis=1).astype(F32)
-    ffn_in = rms_rows(stream, gain[...]).astype(BF16)
-    mine = 4 * t + (row16 & 3) == col16
-    block = jnp.zeros((SEQ, Q), F32)
-    for q in range(NY):
-        pick = jnp.where(mine & ((row16 >> 2) == q), 1.0, 0.0).astype(BF16)
-        block = block + dot(pick, ffn_in[:, q * Q : (q + 1) * Q])
-    xd[x, c, z] = block.astype(BF16)
+    gains = [gain[:, i * 128 : (i + 1) * 128] for i in range(16)]
+    gain8 = jnp.concatenate(
+        [jnp.where(low8, gains[2 * i], gains[2 * i + 1]) for i in range(8)], axis=0
+    ).reshape(1, 8, 8, 128)
     sends = [0]
 
     def give(px, pz, **to):
@@ -287,15 +302,6 @@
 
     def arrive(px, pc, pz):
         landed(xd.at[px, pc, pz], g_r.at[px, pc, pz])
-
-    for k in FAR_FIRST:
-        give(x, z, dz=k)
-    give(x, z, dx=1)
-    give(x, z, dx=-1)
-    give(x, z, flip=1)
-    mix = jax.nn.sigmoid(jnp.sum(ffn_in.astype(F32) * mix_w[...], axis=-1, keepdims=True))
-    mix_row = jnp.sum(jnp.where(eye, jnp.broadcast_to(mix, (SEQ, SEQ)), 0.0), axis=0, keepdims=True)
-    mix_mine = jnp.sum(jnp.where(mine, jnp.broadcast_to(mix_row, (SEQ, SEQ)), 0.0), axis=1, keepdims=True)
 
     def regroup(ref):
         return dot(perm[...], ref[...].reshape(128, Q)).astype(BF16).reshape(8, SEQ, Q)
@@ -307,35 +313,53 @@
         begin(m2s.at[up(z, k, NZ)], my.at[t, z], m2_s.at[k - 1], m2_q.at[k - 1], dz=k)
     my[t, z] = m2s[z]
 
-    for k in Z_ORDER[1:]:
-        pz = up(z, k, NZ)
-        arrive(x, c, pz)
-        give(x, pz, dx=1)
-        give(x, pz, dx=-1)
-        give(x, pz, flip=1)
+    low32 = (lax.broadcasted_iota(jnp.int32, (32, 1), 0) & 7) < 4
+    for ks in (Z_ORDER[:4], Z_ORDER[4:]):
+        for k in ks:
+            for j in range(NY):
+                pz, pt = up(z, k, NZ), up(t, j, NY)
+                if k or j:
+                    landed(raw.at[pz, pt], p_r.at[pz, pt])
+        four = jnp.concatenate([raw[up(z, k, NZ)].reshape(64, 128) for k in ks], axis=0).astype(F32)
+        four = four.reshape(4, 8, 8, 128)
+        square = jnp.sum(four * four, axis=1).reshape(32, 128)
+        square = square + jnp.where(low32, pltpu.roll(square, 28, 0), pltpu.roll(square, 4, 0))
+        mean_sq = jnp.sum(square, axis=1, keepdims=True) * (1.0 / D)
+        root = jnp.broadcast_to(lax.rsqrt(mean_sq + EPS), (32, 128)).reshape(4, 1, 8, 128)
+        ready = (four * root * gain8).reshape(256, 128).astype(BF16)
+        laid = dot(join[...], ready).astype(BF16)
+        wide = jnp.concatenate([laid[j * 64 : (j + 1) * 64] for j in range(4)], axis=1)
+        for i, k in enumerate(ks):
+            pz = up(z, k, NZ)
+            xd[x, c, pz] = wide[i * SEQ : (i + 1) * SEQ]
+            give(x, pz, dx=1)
+            give(x, pz, dx=-1)
+            give(x, pz, flip=1)
 
     loaded("dg", "du", "eg", "eu", *[f"dd{q}" for q in range(NY)])
-    quarter = (lax.broadcasted_iota(jnp.int32, (256, 1), 0) >> 2) & 3
     low_rows = (lax.broadcasted_iota(jnp.int32, (128, 1), 0) & 7) < 4
 
-    def by_quarter(value):
-        return jnp.concatenate(
-            [jnp.where(quarter == q, value, jnp.zeros_like(value)) for q in range(NY)], axis=1
-        )
+    def swapped_rows(value):
+        return jnp.where(low_rows, pltpu.roll(value, 124, 0), pltpu.roll(value, 4, 0))
 
     def dense_rows(k):
         px = up(x, k, NX)
         for pz in range(NZ):
             arrive(px, 1 - c, pz)
-        both = dot(by_quarter(xd[px].reshape(256, Q)), wd[...]).reshape(16, 2, 8, 2 * FF)
-        half = (both[:, 0] + both[:, 1]).reshape(128, 2 * FF)
-        full = half + jnp.where(low_rows, pltpu.roll(half, 124, 0), pltpu.roll(half, 4, 0))
-        hidden = (jax.nn.silu(full[:, 0:FF]) * full[:, FF:]).reshape(16, 8, FF)
-        rows16 = jnp.concatenate([hidden, hidden], axis=1).astype(BF16).reshape(256, FF)
-        part = dot(by_quarter(rows16), ddq[...].reshape(NY * FF, Q))
-        s0[k] = jnp.where(c == 0, part[128:], part[0:128]).astype(BF16)
+        rows = xd[px].reshape(256, Q)
+        part = [dot(rows, wd[q * Q : (q + 1) * Q, :]).reshape(16, 2, 8, 2 * FF) for q in range(NY)]
+        even = (part[0][:, 0] + part[2][:, 1]).reshape(128, 2 * FF)
+        odd = (part[1][:, 0] + part[3][:, 1]).reshape(128, 2 * FF)
+        kept = jnp.where(low_rows, even, odd)
+        full = kept + swapped_rows(kept)
+        hidden = (jax.nn.silu(full[:, 0:FF]) * full[:, FF:]).astype(BF16)
+        got = [dot(hidden, ddq[q]) for q in range(NY)]
+        top = jnp.where(low_rows, got[0], got[1]).reshape(16, 1, 8, Q)
+        bottom = jnp.where(low_rows, got[2], got[3]).reshape(16, 1, 8, Q)
+        added = jnp.concatenate([top, bottom], axis=1).reshape(256, Q)
+        s0[k] = jnp.where(c == 0, added[128:], added[0:128]).astype(BF16)
         begin(s0.at[k], r0.at[k], s0_s.at[k], s0_r.at[k], flip=1)
-        own[k] = jnp.where(c == 0, part[0:128], part[128:])
+        own[k] = jnp.where(c == 0, added[0:128], added[128:])
 
     count = [0]
 
@@ -360,6 +384,8 @@
                 give(px, pz, dx=way)
             give(px, pz, flip=1)
     dense_rows(0)
+    dense_rows(1)
+    dense_rows(3)
     for m, k in enumerate(Z_ORDER):
         pz = up(z, k, NZ)
         for way in (1, -1):
@@ -367,13 +393,11 @@
             landed(my.at[pt, pz], my_r.at[pt, pz])
             if (m % 2 == 0) == (way == 1):
                 pass_on(pt, pz, way)
-    dense_rows(1)
     for k in Z_ORDER:
         pz = up(z, k, NZ)
         px = up(x, 2, NX)
         arrive(px, c, pz)
         give(px, pz, flip=1)
-    dense_rows(3)
 
     left = slice(0, Q // 2)
     right = slice(Q // 2, Q)
@@ -435,6 +459,15 @@
     for k in FAR_FIRST:
         begin(s2.at[up(z, k, NZ)], r2.at[k - 1], s2_s.at[k - 1], s2_r.at[k - 1], dz=k)
 
+    for k in (1, 3, 2):
+        src = up(t, -k, NY)
+        landed(sg.at[src], c_r.at[k - 1])
+    stream = jnp.concatenate([sg[k] for k in range(NY)], axis=1).astype(F32)
+    ffn_in = rms_rows(stream, gain[...]).astype(BF16)
+    mine = 4 * t + (row16 & 3) == col16
+    mix = jax.nn.sigmoid(jnp.sum(ffn_in.astype(F32) * mix_w[...], axis=-1, keepdims=True))
+    mix_row = jnp.sum(jnp.where(eye, jnp.broadcast_to(mix, (SEQ, SEQ)), 0.0), axis=0, keepdims=True)
+    mix_mine = jnp.sum(jnp.where(mine, jnp.broadcast_to(mix_row, (SEQ, SEQ)), 0.0), axis=1, keepdims=True)
     for k in reversed(FAR_FIRST):
         landed(n1r.at[up(z, -k, NZ)], n1_q.at[k - 1])
     n2s[...] = regroup(n1r)
@@ -521,6 +554,10 @@
             buf((8, SEQ, Q)),
             buf((8, SEQ, Q)),
             buf((NX, NC, NZ, SEQ, Q)),
+            buf((4, 64, SEQ)),
+            buf((256, 256)),
+            buf((NY, SEQ, 128)),
+            buf((NZ, NY, SEQ, 128)),
             buf((NX, NZ * SEQ, Q)),
             buf((NX, NZ * SEQ, Q)),
             buf((NX, NZ * SEQ, Q), F32),
@@ -533,7 +570,7 @@
             buf((NY, 8, Q), F32),
             dma(27),
             dma(3), dma(3), dma(3), dma(3), dma(3), dma(3), dma(3), dma(3), dma(3), dma(3),
-            dma(N_SENDS), dma(NX, NC, NZ),
+            dma(N_SENDS), dma(NX, NC, NZ), dma(31), dma(NZ, NY),
             dma(7), dma(7), dma(7), dma(7),
             dma(24), dma(NY, NZ),
             dma(7), dma(7), dma(7), dma(7),

time: 56.6 us -> 54.7 us (0.966)
  Pallas kernels: 54.2 us -> 52.7 us
    pallas_call x1, Pallas kernels: 54.2 us -> 52.7 us  [layer(): pl.pallas_call(layer_kernel, out_shape=(pltpu.VMEM((SEQ, Q), F32), pltpu....]
where the time goes in v6:
time: 54.7 us; the launch traced here: 54.6 us
  Pallas kernels  52.7 us (96%)
  between operations  0.65 us (1%)
  other arithmetic  0.61 us (1%)
  local copies, waits for them, and re-layouts  0.6 us (1%)
    pallas_call x1, Pallas kernels, layer(): pl.pallas_call(layer_kernel, out_shape=(pltpu.VMEM((SEQ, Q), F32), pltpu....  52.7 us

profile of v6, /device:TPU:1, one launch (start us, length us, event | category | flops | bytes accessed | tf_op | source)
XLA Modules:
  0.0 54.6 jit_solution(58695712415986467)
XLA Ops:
  0.6 52.7 %layer.1 = (f32[16,512]{1,0:T(8,128)S(1)}, bf16[16,256]{1,0:T(8,128)(2,1)S(1)}) custom-call(bf16[16,2048]{1,0:T(8,128)(2,1)} %resid_h.1, s32[1,16]{1,0:T(1,128)} %bitcast.23, bf16[16,512,256]{2,1,0:T(8,128)(2,1)} %bitcast.14, f32[1,2048]{1,0:T(1,128)} %bitcast.18, bf16[2048,512]{1,0:T(8,128)(2,1)} %wq_h.1, bf16[2048,128]{1,0:T(8,128)(2,1)} %wk_h.1, ...), custom_call_target="tpu_custom_call" | custom-call | tf_op jit(solution)/shard_map/layer/pallas_call | solution.py:511
  53.3 0.6 %convert_element_type.3 = bf16[16,512]{1,0:T(8,128)(2,1)} convert(f32[16,512]{1,0:T(8,128)S(1)} %get-tuple-element.4) | non-fusion elementwise | flops 8192 | bytes 49152 | tf_op jit(solution)/shard_map/convert_element_type | solution.py:618
  54.0 0.6 %copy.24 = bf16[16,1,256]{2,0,1:T(8,128)(2,1)} copy(bf16[16,1,256]{2,0,1:T(8,128)(2,1)S(1)} %bitcast.13) | data formatting | bytes 16384
